TPU v7x, 32 devices: a whole 2x2x4 slice. The times are simulated.
32 devices in a mesh: ep: 8 (over z, x), tp: 4 (over y, core).
Axes of the slice: x: 2, y: 2, z: 4, core: 2. Of those that a mesh axis runs over, the one named last changes fastest.
Arguments:
- query_latent: bfloat16 [4096, 768], P(('ep', 'tp')), may hold values from -6 to 6
- kv_latent: bfloat16 [4096, 512], P(('ep', 'tp')), may hold values from -6 to 6
- rope_key: bfloat16 [4096, 64], P(('ep', 'tp')), may hold values from -6 to 6
- query_gain: float32 [768], replicated, may hold values from 0.1 to 12
- kv_gain: float32 [512], replicated, may hold values from 0.1 to 12
- query_nope_w: bfloat16 [768, 1024], P(None, 'tp'), may hold values from -0.21875 to 0.21875
- query_rope_w: bfloat16 [768, 512], P(None, 'tp'), may hold values from -0.21875 to 0.21875
- key_up_w: bfloat16 [512, 1024], P(None, 'tp'), may hold values from -0.25 to 0.25
- value_up_w: bfloat16 [512, 1024], P(None, 'tp'), may hold values from -0.25 to 0.25
- output_w: bfloat16 [1024, 2048], P('tp'), may hold values from -0.1875 to 0.1875
- expert_in: bfloat16 [4096, 2048], P(('ep', 'tp')), may hold values from -6 to 6
- moe_gain: float32 [2048], replicated, may hold values from 0.1 to 12
- routes: int32 [4096, 2], P(('ep', 'tp')), may hold values from 0 to 15, all different within a row; in each aligned block of 128 rows (0 to 127, 128 to 255, ...) at most 20 rows name the same one
- route_weight: float32 [4096, 2], P(('ep', 'tp')), may hold values from 0.1 to 1
- gate_w: bfloat16 [16, 2048, 2048], P('ep', None, 'tp'), may hold values from -0.125 to 0.125
- up_w: bfloat16 [16, 2048, 2048], P('ep', None, 'tp'), may hold values from -0.125 to 0.125
- down_w: bfloat16 [16, 2048, 2048], P('ep', 'tp'), may hold values from -0.125 to 0.125
Outputs:
- mixer_out: bfloat16 [4096, 2048], P(('ep', 'tp'))
- expert_out: bfloat16 [4096, 2048], P(('ep', 'tp'))
Inputs may be any that keep to these rules, and one draw needn't show every extreme that they name: `routes`: each row names 2 different experts; in the rows of one device no expert is named more than 20 times.
All inputs are finite; a program needn't handle non-finite values.
Results may differ from a plain program's by a relative error of at most 0.015.
The roundings to bfloat16 on the way count: a program that leaves them out, or rounds other values in their place, can miss the bound.
Values may be sent and summed in bfloat16 or wider, within the bound.
A program may use at most 128 MiB of HBM per device.

v0:
```python
import functools
import math

import jax
import jax.numpy as jnp
from jax import lax
from jax.experimental import pallas as pl
from jax.experimental.pallas import tpu as pltpu
from jax.sharding import PartitionSpec as P

NOPE = 128


THETA = 10000.0

PAD = 256

NT = (((1,), (1,)), ((), ()))


def rms_scale(values, gain):
    floats = values.astype(jnp.float32)
    square = jnp.mean(floats * floats, axis=-1, keepdims=True)
    return (floats * lax.rsqrt(square + 1e-06) * gain).astype(jnp.bfloat16)


def attend_kernel(heads, rope, last_ref, lat_ref, q_ref, wk_ref, wv_ref, out_ref, peak, total, acc):
    rows = q_ref.shape[0]
    vdim = wv_ref.shape[0] // heads
    scale = math.log2(math.e) / math.sqrt(NOPE + rope)
    peak[...] = jnp.full_like(peak, -1e30)
    total[...] = jnp.zeros_like(total)
    acc[...] = jnp.zeros_like(acc)

    def block(number, masked):
        lat = lat_ref[pl.ds(pl.multiple_of(number * rows, rows), rows), :]
        keys = jnp.dot(lat, wk_ref[...], preferred_element_type=jnp.float32).astype(jnp.bfloat16)
        vals = lax.dot_general(
            wv_ref[...], lat, NT, preferred_element_type=jnp.float32
        ).astype(jnp.bfloat16)
        for h in range(heads):
            score = (
                lax.dot_general(
                    keys[:, h * PAD : (h + 1) * PAD],
                    q_ref[:, h * PAD : (h + 1) * PAD],
                    NT,
                    preferred_element_type=jnp.float32,
                )
                * scale
            )
            if masked:
                key = lax.broadcasted_iota(jnp.int32, score.shape, 0)
                query = lax.broadcasted_iota(jnp.int32, score.shape, 1)
                score = jnp.where(key <= query, score, -1e30)
            old = peak[h : h + 1, :]
            new = jnp.maximum(old, jnp.max(score, axis=0, keepdims=True))
            expo = jnp.exp2(score - new)
            factor = jnp.exp2(old - new)
            peak[h : h + 1, :] = new
            total[h : h + 1, :] = total[h : h + 1, :] * factor + jnp.sum(
                expo, axis=0, keepdims=True
            )
            part = slice(h * vdim, (h + 1) * vdim)
            acc[part, :] = acc[part, :] * factor + jnp.dot(
                vals[part, :], expo.astype(jnp.bfloat16), preferred_element_type=jnp.float32
            )

    last = last_ref[0]

    @pl.loop(0, last)
    def _(number):
        block(number, False)

    block(last, True)
    for h in range(heads):
        part = slice(h * vdim, (h + 1) * vdim)
        out_ref[part, :] = (acc[part, :] / total[h : h + 1, :]).astype(jnp.bfloat16)


def attend(last, latents, queries, key_w, value_w, heads, rope):
    rows = queries.shape[0]
    vdim_all = value_w.shape[0]
    vmem = pl.BlockSpec(memory_space=pltpu.VMEM)
    length = latents.shape[0]
    return pl.pallas_call(
        functools.partial(attend_kernel, heads, rope),
        out_shape=jax.ShapeDtypeStruct((vdim_all, rows), jnp.bfloat16),
        in_specs=[pl.BlockSpec(memory_space=pltpu.SMEM)] + [vmem] * 4,
        out_specs=vmem,
        scratch_shapes=[
            pltpu.VMEM((heads, rows), jnp.float32),
            pltpu.VMEM((heads, rows), jnp.float32),
            pltpu.VMEM((vdim_all, rows), jnp.float32),
        ],
        compiler_params=pltpu.CompilerParams(vmem_limit_bytes=40 * 1024 * 1024),
        cost_estimate=pl.CostEstimate(
            flops=2 * length * rows * heads * (PAD + 2 * NOPE),
            bytes_accessed=latents.size * 2,
            transcendentals=length * rows * heads,
        ),
    )(last, latents, queries, key_w, value_w)


def mixer_front(query_latent, kv_latent, rope_key, query_gain, kv_gain):
    tok_rows = query_latent.shape[0]
    rope = rope_key.shape[1]
    half = rope // 2
    group_rows = tok_rows * lax.axis_size("tp")
    freq = 1.0 / THETA ** (jnp.arange(half, dtype=jnp.float32) * 2.0 / rope)
    first_pos = lax.axis_index("ep") * group_rows
    positions = first_pos + jnp.arange(group_rows, dtype=jnp.int32)
    own = lax.axis_index("tp") * tok_rows + first_pos + jnp.arange(tok_rows, dtype=jnp.int32)
    angle = own.astype(jnp.float32)[:, None] * jnp.tile(freq, 2)[None, :]
    keys = rope_key.astype(jnp.float32)
    turned = jnp.concatenate([-keys[:, half:], keys[:, :half]], axis=-1)
    key_rot = (keys * jnp.cos(angle) + turned * jnp.sin(angle)).astype(jnp.bfloat16)
    kv_normed = rms_scale(kv_latent, kv_gain)
    own_latents = jnp.concatenate([kv_normed, key_rot], axis=1)
    query_normed = lax.all_gather(rms_scale(query_latent, query_gain), "tp", axis=0, tiled=True)
    return own_latents, query_normed, positions, freq


def mixer(
    front, rope, query_nope_w, query_rope_w, key_up_w, value_up_w, output_w
):
    latents, query_normed, positions, freq = front
    half = rope // 2
    heads = query_nope_w.shape[1] // NOPE
    kv_width = key_up_w.shape[0]
    angle = positions.astype(jnp.float32)[:, None] * jnp.tile(freq, 2 * heads)[None, :]
    turned_w = []
    for h in range(heads):
        turned_w.append(-query_rope_w[:, h * rope + half : (h + 1) * rope])
        turned_w.append(query_rope_w[:, h * rope : h * rope + half])
    weights = jnp.concatenate([query_nope_w, query_rope_w] + turned_w, axis=1)
    flat = jnp.dot(query_normed, weights, preferred_element_type=jnp.float32)
    nope_all = heads * NOPE
    rope_all = heads * rope
    rot = (
        flat[:, nope_all : nope_all + rope_all] * jnp.cos(angle)
        + flat[:, nope_all + rope_all :] * jnp.sin(angle)
    ).astype(jnp.bfloat16)
    query_flat = flat[:, :nope_all].astype(jnp.bfloat16)
    blank = jnp.zeros((flat.shape[0], PAD - NOPE - rope), jnp.bfloat16)
    pieces = []
    for h in range(heads):
        pieces += [
            query_flat[:, h * NOPE : (h + 1) * NOPE],
            rot[:, h * rope : (h + 1) * rope],
            blank,
        ]
    queries = jnp.concatenate(pieces, axis=1)
    carry = jnp.pad(
        jnp.eye(rope, dtype=jnp.bfloat16), ((0, 0), (NOPE, PAD - NOPE - rope))
    )
    key_w = jnp.concatenate(
        [
            jnp.concatenate(
                [
                    jnp.pad(key_up_w[:, h * NOPE : (h + 1) * NOPE], ((0, 0), (0, PAD - NOPE))),
                    carry,
                ],
                axis=0,
            )
            for h in range(heads)
        ],
        axis=1,
    )
    value_w = jnp.pad(value_up_w.T, ((0, 0), (0, latents.shape[1] - kv_width)))
    last = lax.axis_index("ep").astype(jnp.int32).reshape(1)
    attended = attend(last, latents, queries, key_w, value_w, heads, rope)
    mixed = lax.dot_general(
        attended, output_w, (((0,), (0,)), ((), ())), preferred_element_type=jnp.float32
    ).astype(jnp.bfloat16)
    return lax.psum_scatter(mixed, "tp", scatter_dimension=0, tiled=True)


def route(routes, experts, local, capacity):
    rows = routes.shape[0]
    main = capacity // 8 * 8
    rest = capacity - main
    names = jnp.arange(experts, dtype=jnp.int32)[None, :]
    chosen = [routes[:, k : k + 1] == names for k in range(routes.shape[1])]
    member = functools.reduce(jnp.logical_or, chosen).astype(jnp.bfloat16)
    before = lax.broadcasted_iota(jnp.int32, (rows, rows), 0) > lax.broadcasted_iota(
        jnp.int32, (rows, rows), 1
    )
    rank = jnp.dot(
        before.astype(jnp.bfloat16), member, preferred_element_type=jnp.float32
    ).astype(jnp.int32)
    inner = names % local
    place = jnp.where(
        rank < main, inner * main + rank, local * main + inner * rest + rank - main
    ) + names // local * (local * capacity)
    slots = lax.broadcasted_iota(jnp.int32, (rows, experts * capacity), 1)
    return [
        jnp.sum(jnp.where(one, place, 0), axis=1, keepdims=True) == slots for one in chosen
    ]


def swap(values, bit):
    size = lax.axis_size("tp")
    return lax.ppermute(values, "tp", [(one, one ^ bit) for one in range(size)])


def expert_rows(pieces, local, main, rest, gate_w, up_w, down_w):
    groups, piece, width = pieces.shape
    mixed = pieces[:, local * main :].reshape(groups * local * rest, width)
    owner = (
        lax.broadcasted_iota(jnp.int32, (groups * local * rest, 1), 0) % (local * rest)
    ) // max(rest, 1)
    mains = []
    shared = 0.0
    for expert in range(local):
        inputs = jnp.concatenate(
            [
                pieces[:, expert * main : (expert + 1) * main].reshape(groups * main, width),
                mixed,
            ],
            axis=0,
        )
        gate = jnp.minimum(jnp.dot(inputs, gate_w[expert], preferred_element_type=jnp.float32), 7.0)
        upper = jnp.clip(
            jnp.dot(inputs, up_w[expert], preferred_element_type=jnp.float32), -7.0, 7.0
        )
        hidden = (gate * jax.nn.sigmoid(1.702 * gate) * (upper + 1.0)).astype(jnp.bfloat16)
        output = jnp.dot(hidden, down_w[expert], preferred_element_type=jnp.float32).astype(
            jnp.bfloat16
        )
        mains.append(output[: groups * main].reshape(groups, main, width))
        shared = jnp.where(owner == expert, output[groups * main :], shared)
    shared = shared.astype(jnp.bfloat16).reshape(groups, local * rest, width)
    return jnp.concatenate(mains + [shared], axis=1)


def add_rounded(one, other):
    return (one.astype(jnp.float32) + other.astype(jnp.float32)).astype(jnp.bfloat16)


def group_experts(arrived, run):
    size = lax.axis_size("tp")
    if size & (size - 1):
        spread = lax.all_gather(arrived, "tp", axis=0, tiled=True)
        return lax.psum_scatter(run(spread), "tp", scatter_dimension=0, tiled=True)
    count = arrived.shape[0]
    far = {0: arrived}
    for bit in [1 << k for k in range(1, size.bit_length() - 1)]:
        for key in sorted(far):
            far[key | bit] = swap(far[key], bit)
    results = {}
    for key in sorted(far):
        if size == 1:
            results[key] = run(far[key])
            continue
        near = swap(far[key], 1)
        both = run(jnp.concatenate([far[key], near], axis=0))
        results[key] = add_rounded(both[:count], swap(both[count:], 1))
    for bit in [1 << k for k in range(size.bit_length() - 2, 0, -1)]:
        for key in sorted(results):
            if key & bit:
                results[key ^ bit] = add_rounded(results[key ^ bit], swap(results.pop(key), bit))
    return results[0]


def experts_half(expert_in, moe_gain, routes, route_weight, gate_w, up_w, down_w, tied):
    tok_rows, top_count = routes.shape
    width = expert_in.shape[1]
    local = gate_w.shape[0]
    ep_size = lax.axis_size("ep")
    experts = local * ep_size
    capacity = max(2, 5 * tok_rows * top_count // (4 * experts))
    main = capacity // 8 * 8
    rest = capacity - main
    piece = local * capacity
    floats = expert_in.astype(jnp.float32)
    center = floats - jnp.mean(floats, axis=-1, keepdims=True)
    variance = jnp.mean(center * center, axis=-1, keepdims=True)
    normed_in = (center * lax.rsqrt(variance + 1e-05) * moe_gain).astype(jnp.bfloat16)
    hits = route(routes, experts, local, capacity)
    select = functools.reduce(jnp.logical_or, hits).astype(jnp.bfloat16)
    outgoing = lax.dot_general(
        select, normed_in, (((0,), (0,)), ((), ())), preferred_element_type=jnp.float32
    ).astype(jnp.bfloat16)
    outgoing, tied = lax.optimization_barrier((outgoing, tied))
    latents = lax.all_gather(tied, ("ep", "tp"), axis=0, tiled=True)
    outgoing = outgoing.reshape(ep_size, piece, width)
    arrived = lax.all_to_all(outgoing, "ep", split_axis=0, concat_axis=0, tiled=True)
    summed = group_experts(
        arrived,
        lambda pieces: expert_rows(pieces, local, main, rest, gate_w, up_w, down_w),
    )
    back = lax.all_to_all(summed, "ep", split_axis=0, concat_axis=0, tiled=True).reshape(
        experts * capacity, width
    )
    weights = route_weight / jnp.sum(route_weight, axis=-1, keepdims=True)
    mix = sum(jnp.where(hit, weights[:, k : k + 1], 0.0) for k, hit in enumerate(hits))
    high = mix.astype(jnp.bfloat16)
    low = (mix - high.astype(jnp.float32)).astype(jnp.bfloat16)
    both = jnp.dot(
        jnp.concatenate([high, low], axis=0), back, preferred_element_type=jnp.float32
    )
    return (both[:tok_rows] + both[tok_rows:]).astype(jnp.bfloat16), latents


def per_device(
    query_latent,
    kv_latent,
    rope_key,
    query_gain,
    kv_gain,
    query_nope_w,
    query_rope_w,
    key_up_w,
    value_up_w,
    output_w,
    expert_in,
    moe_gain,
    routes,
    route_weight,
    gate_w,
    up_w,
    down_w,
):
    front = mixer_front(query_latent, kv_latent, rope_key, query_gain, kv_gain)
    expert_out, latents = experts_half(
        expert_in, moe_gain, routes, route_weight, gate_w, up_w, down_w, front[0]
    )
    mixer_out = mixer(
        (latents,) + front[1:],
        rope_key.shape[1],
        query_nope_w,
        query_rope_w,
        key_up_w,
        value_up_w,
        output_w,
    )
    return (mixer_out, expert_out)


def solution(mesh):
    placed = (
        P(("ep", "tp"), None),
        P(("ep", "tp"), None),
        P(("ep", "tp"), None),
        P(),
        P(),
        P(None, "tp"),
        P(None, "tp"),
        P(None, "tp"),
        P(None, "tp"),
        P("tp", None),
        P(("ep", "tp"), None),
        P(),
        P(("ep", "tp"), None),
        P(("ep", "tp"), None),
        P("ep", None, "tp"),
        P("ep", None, "tp"),
        P("ep", "tp", None),
    )
    return jax.shard_map(
        per_device,
        mesh=mesh,
        in_specs=placed,
        out_specs=(P(("ep", "tp"), None), P(("ep", "tp"), None)),
        check_vma=False,
    )
```

profile of v0, /device:TPU:0, one launch (start us, length us, event | category | flops | bytes accessed | tf_op | source)
XLA Modules:
  0.0 249.6 jit_solution(1583856517357572293)
XLA Ops:
  7.2 0.9 copy.19
  8.2 0.8 slice_bitcast_fusion.5
  9.0 1.2 convert_reduce_fusion
  10.2 1.3 fusion.97
  11.7 1.0 fusion.162
  12.7 1.0 fusion.164
  15.0 1.8 convolution_convert_fusion.5
  16.7 7.4 %all-to-all-start = ((bf16[8,40,2048]{2,1,0:T(8,128)(2,1)}), bf16[8,40,2048]{2,1,0:T(8,128)(2,1)S(1)}, u32[]{:S(2)}, u32[]{:S(2)}) async-start(bf16[8,40,2048]{2,1,0:T(8,128)(2,1)} %bitcast.112), calls=%async_computation.1 | async-start | bytes 2621440 | tf_op jit(solution)/shard_map/all_to_all | solution.py:287
  25.2 33.8 %all-to-all-done = bf16[8,40,2048]{2,1,0:T(8,128)(2,1)S(1)} async-done(((bf16[8,40,2048]{2,1,0:T(8,128)(2,1)}), bf16[8,40,2048]{2,1,0:T(8,128)(2,1)S(1)}, u32[]{:S(2)}, u32[]{:S(2)}) %all-to-all-start) | async-done | bytes 1310752 | tf_op jit(solution)/shard_map/all_to_all | solution.py:287
  59.0 1.0 fusion.221
  60.0 11.8 %all_gather.7 = bf16[512,768]{1,0:T(8,128)(2,1)} all-gather(bf16[128,768]{1,0:T(8,128)(2,1)S(1)} %fusion.145), channel_id=1, replica_groups=mesh['ep'=8,'tp'=4] {'tp'}, dimensions={0}, use_global_device_ids=true | all-gather | bytes 983040 | tf_op jit(solution)/shard_map/all_gather | solution.py:119
  71.9 1.4 collective-permute-start.2
  73.9 2.3 concatenate.50
  76.2 2.8 %fusion.223 = (bf16[512,512]{1,0:T(8,128)(2,1)}, f32[512,512]{1,0:T(8,128)}) fusion(bf16[512,768]{1,0:T(8,128)(2,1)} %all_gather.7, bf16[768,512]{1,0:T(8,128)(2,1)S(1)} %concatenate.50), kind=kOutput, calls=%fused_computation.246 | convolution fusion | flops 402915328 | bytes 3145728 | tf_op jit(solution)/shard_map/dot_general | solution.py:136
  79.1 1.4 constant_dynamic-update-slice_fusion
  80.6 31.7 %collective-permute-done.2 = bf16[8,40,2048]{2,1,0:T(8,128)(2,1)} collective-permute-done((bf16[8,40,2048]{2,1,0:T(8,128)(2,1)S(1)}, bf16[8,40,2048]{2,1,0:T(8,128)(2,1)}, u32[]{:S(2)}, u32[]{:S(2)}) %collective-permute-start.2) | collective-permute-done | bytes 1310752 | tf_op jit(solution)/shard_map/ppermute | solution.py:203
  112.5 1.9 fusion.50
  114.4 1.9 fusion.44
  116.3 2.6 %constant_dynamic-update-slice_fusion.3 = bf16[16,40,2048]{2,1,0:T(8,128)(2,1)} fusion(bf16[8,40,2048]{2,1,0:T(8,128)(2,1)} %collective-permute-done.2), kind=kLoop, calls=%fused_computation.180 | loop fusion | bytes 2621440
  118.8 6.1 %convolution_convert_fusion.3 = bf16[384,2048]{1,0:T(8,128)(2,1)} fusion(bf16[2,512,2048]{2,1,0:T(8,128)(2,1)} %param.33, bf16[2,2048,512]{2,1,0:T(8,128)(2,1)} %param.32, bf16[128,2048]{1,0:T(8,128)(2,1)} %copy-done.13, bf16[256,2048]{1,0:T(8,128)(2,1)} %bitcast.123, f32[384,512]{1,0:T(8,128)} %fusion.50), kind=kOutput, calls=%fused_computation.3 | convolution fusion | flops 1616314368 | bytes 8126464 | tf_op jit(solution)/shard_map/dot_general | solution.py:227
  124.9 5.8 %convolution_convert_fusion.4 = bf16[384,2048]{1,0:T(8,128)(2,1)} fusion(bf16[2,512,2048]{2,1,0:T(8,128)(2,1)} %param.33, bf16[2,2048,512]{2,1,0:T(8,128)(2,1)} %param.32, bf16[128,2048]{1,0:T(8,128)(2,1)} %copy-done.13, bf16[256,2048]{1,0:T(8,128)(2,1)S(1)} %bitcast.119, f32[384,512]{1,0:T(8,128)} %fusion.44), kind=kOutput, calls=%fused_computation.4 | convolution fusion | flops 1616314368 | bytes 8126464 | tf_op jit(solution)/shard_map/dot_general | solution.py:227
  130.7 1.2 constant_dynamic-update-slice_fusion.2
  131.9 1.1 slice_bitcast_fusion
  133.0 1.9 fusion.219
  134.9 1.1 copy-done.24
  136.0 1.9 fusion.53
  137.9 5.7 %convolution_convert_fusion.1 = bf16[384,2048]{1,0:T(8,128)(2,1)} fusion(bf16[2,512,2048]{2,1,0:T(8,128)(2,1)} %param.33, bf16[2,2048,512]{2,1,0:T(8,128)(2,1)} %param.32, bf16[128,2048]{1,0:T(8,128)(2,1)} %copy-done.14, bf16[256,2048]{1,0:T(8,128)(2,1)S(1)} %bitcast.125, f32[384,512]{1,0:T(8,128)} %fusion.53), kind=kOutput, calls=%fused_computation.1 | convolution fusion | flops 1616314368 | bytes 8126464 | tf_op jit(solution)/shard_map/dot_general | solution.py:227
  143.6 1.4 slice.205
  144.9 3.5 %fusion.47 = f32[384,512]{1,0:T(8,128)} fusion(bf16[2,2048,512]{2,1,0:T(8,128)(2,1)} %param.31, bf16[128,2048]{1,0:T(8,128)(2,1)S(1)} %copy-done.15, bf16[256,2048]{1,0:T(8,128)(2,1)S(1)} %bitcast.120), kind=kOutput, calls=%fused_computation.54 | convolution fusion | flops 808648704 | bytes 4456448 | tf_op jit(solution)/shard_map/dot_general | solution.py:222
  148.4 5.8 %convolution_convert_fusion.2 = bf16[384,2048]{1,0:T(8,128)(2,1)} fusion(bf16[2,512,2048]{2,1,0:T(8,128)(2,1)} %param.33, bf16[2,2048,512]{2,1,0:T(8,128)(2,1)} %param.32, bf16[128,2048]{1,0:T(8,128)(2,1)} %copy-done.14, bf16[256,2048]{1,0:T(8,128)(2,1)S(1)} %bitcast.121, f32[384,512]{1,0:T(8,128)} %fusion.47), kind=kOutput, calls=%fused_computation.2 | convolution fusion | flops 1616314368 | bytes 8126464 | tf_op jit(solution)/shard_map/dot_general | solution.py:227
  154.2 1.4 copy-done.7
  155.6 1.5 fusion.139
  157.5 1.6 copy-done.2
  159.1 1.2 slice.209
  160.8 1.1 fusion.167
  163.1 1.2 slice-done.1
  164.9 1.2 slice.200
  166.4 1.6 copy-done.3
  168.1 2.9 %add_convert_fusion.1 = bf16[8,40,2048]{2,1,0:T(8,128)(2,1)} fusion(bf16[8,40,2048]{2,1,0:T(8,128)(2,1)} %collective-permute-done.4, bf16[16,40,2048]{2,1,0:T(8,128)(2,1)S(1)} %copy-done.3), kind=kLoop, calls=%fused_computation.9 | loop fusion | flops 2621440 | bytes 3932160 | tf_op jit(solution)/shard_map/convert_element_type | solution.py:237
  171.0 1.4 collective-permute-start.5
  172.5 2.5 copy-done.1
  174.9 1.7 shard_map.176
  176.7 2.1 convolution_convert_fusion
  178.8 23.5 %collective-permute-done.5 = bf16[8,40,2048]{2,1,0:T(8,128)(2,1)} collective-permute-done((bf16[8,40,2048]{2,1,0:T(8,128)(2,1)}, bf16[8,40,2048]{2,1,0:T(8,128)(2,1)}, u32[]{:S(2)}, u32[]{:S(2)}) %collective-permute-start.5) | collective-permute-done | bytes 1310752 | tf_op jit(solution)/shard_map/ppermute | solution.py:203
  202.3 3.9 %add_convert_fusion = bf16[8,40,2048]{2,1,0:T(8,128)(2,1)} fusion(bf16[8,40,2048]{2,1,0:T(8,128)(2,1)} %collective-permute-done.5, bf16[8,40,2048]{2,1,0:T(8,128)(2,1)} %collective-permute-done.1, bf16[16,40,2048]{2,1,0:T(8,128)(2,1)} %copy-done.4), kind=kLoop, calls=%fused_computation.8 | loop fusion | flops 5242880 | bytes 5242880 | tf_op jit(solution)/shard_map/convert_element_type | solution.py:237
  206.2 3.7 %all-to-all-start.1 = ((bf16[8,40,2048]{2,1,0:T(8,128)(2,1)}), bf16[8,40,2048]{2,1,0:T(8,128)(2,1)S(1)}, u32[]{:S(2)}, u32[]{:S(2)}) async-start(bf16[8,40,2048]{2,1,0:T(8,128)(2,1)} %add_convert_fusion), calls=%async_computation.2 | async-start | bytes 2621440 | tf_op jit(solution)/shard_map/all_to_all | solution.py:292
  210.1 31.0 %all-to-all-done.1 = bf16[8,40,2048]{2,1,0:T(8,128)(2,1)S(1)} async-done(((bf16[8,40,2048]{2,1,0:T(8,128)(2,1)}), bf16[8,40,2048]{2,1,0:T(8,128)(2,1)S(1)}, u32[]{:S(2)}, u32[]{:S(2)}) %all-to-all-start.1) | async-done | bytes 1310752 | tf_op jit(solution)/shard_map/all_to_all | solution.py:292
  241.8 0.9 fusion.100
  (108 shorter events, 7.2 us)
Async XLA Ops:
  7.2 169.5 %copy-start = (bf16[256,2048]{1,0:T(8,128)(2,1)S(1)}, bf16[256,2048]{1,0:T(8,128)(2,1)}, u32[]{:S(2)}) copy-start(bf16[256,2048]{1,0:T(8,128)(2,1)} %param.26) | copy-start | bytes 3145732
  7.2 7.7 %copy-start.6 = (bf16[128,2048]{1,0:T(8,128)(2,1)S(1)}, bf16[128,2048]{1,0:T(8,128)(2,1)}, u32[]{:S(2)}) copy-start(bf16[128,2048]{1,0:T(8,128)(2,1)} %param.27) | copy-start | bytes 1572868
  7.2 7.7 %copy-start.17 = (f32[2048]{0:T(1024)S(1)}, f32[2048]{0:T(1024)}, u32[]{:S(2)}) copy-start(f32[2048]{0:T(1024)} %param.28) | copy-start | bytes 24580
  14.9 10.0 %copy-start.11 = (bf16[128,768]{1,0:T(8,128)(2,1)S(1)}, bf16[128,768]{1,0:T(8,128)(2,1)}, u32[]{:S(2)}) copy-start(bf16[128,768]{1,0:T(8,128)(2,1)} %param.17) | copy-start | bytes 589828
  14.9 10.1 %copy-start.18 = (f32[768]{0:T(1024)S(1)}, f32[768]{0:T(1024)}, u32[]{:S(2)}) copy-start(f32[768]{0:T(1024)} %param.20) | copy-start | bytes 9220
  16.7 42.3 %copy-start.5 = (bf16[768,128]{1,0:T(8,128)(2,1)S(1)}, bf16[768,128]{1,0:T(8,128)(2,1)}, u32[]{:S(2)}) copy-start(bf16[768,128]{1,0:T(8,128)(2,1)} %param.23) | copy-start | bytes 589828
  16.7 42.3 %all-to-all-start = ((bf16[8,40,2048]{2,1,0:T(8,128)(2,1)}), bf16[8,40,2048]{2,1,0:T(8,128)(2,1)S(1)}, u32[]{:S(2)}, u32[]{:S(2)}) async-start(bf16[8,40,2048]{2,1,0:T(8,128)(2,1)} %bitcast.112), calls=%async_computation.1 | async-start | bytes 2621440 | tf_op jit(solution)/shard_map/all_to_all | solution.py:287
  24.1 148.3 %all-gather.2.cloned.1.call-start = ((), (), s32[]{:S(2)}) async-start(), calls=%async_computation.3 | async-start | bytes 5406720 | tf_op jit(solution)/shard_map/all_gather | solution.py:285
  24.9 217.9 %reduce-scatter.2.cloned.1.call-start = ((), (), s32[]{:S(2)}) async-start(), calls=%async_computation.4 | async-start | bytes 2621440 | tf_op jit(solution)/shard_map/reduce_scatter | solution.py:175
  59.0 20.1 %collective-permute-start = (bf16[8,40,2048]{2,1,0:T(8,128)(2,1)S(1)}, bf16[8,40,2048]{2,1,0:T(8,128)(2,1)}, u32[]{:S(2)}, u32[]{:S(2)}) collective-permute-start(bf16[8,40,2048]{2,1,0:T(8,128)(2,1)S(1)} %all-to-all-done), channel_id=1, source_target_pairs={{0,1},{1,0},{2,3},{3,2},{4,5},{5,4},{6,7},{7,6},{8,9},{9,8},{10,11... | collective-permute-start | bytes 3932168 | tf_op jit(solution)/shard_map/ppermute | solution.py:203
  71.9 40.4 %collective-permute-start.2 = (bf16[8,40,2048]{2,1,0:T(8,128)(2,1)S(1)}, bf16[8,40,2048]{2,1,0:T(8,128)(2,1)}, u32[]{:S(2)}, u32[]{:S(2)}) collective-permute-start(bf16[8,40,2048]{2,1,0:T(8,128)(2,1)S(1)} %all-to-all-done), channel_id=1, source_target_pairs={{0,2},{1,3},{2,0},{3,1},{4,6},{5,7},{6,4},{7,5},{8,10},{9,11},{10,... | collective-permute-start | bytes 3932168 | tf_op jit(solution)/shard_map/ppermute | solution.py:203
  80.6 33.8 %copy-start.13 = (bf16[128,2048]{1,0:T(8,128)(2,1)}, bf16[128,2048]{1,0:T(8,128)(2,1)S(1)}, u32[]{:S(2)}) copy-start(bf16[128,2048]{1,0:T(8,128)(2,1)S(1)} %slice_bitcast_fusion.1) | copy-start | bytes 1572868
  80.6 31.9 %copy-start.23 = (bf16[2,2048,512]{2,1,0:T(8,128)(2,1)S(1)}, bf16[2,2048,512]{2,1,0:T(8,128)(2,1)}, u32[]{:S(2)}) copy-start(bf16[2,2048,512]{2,1,0:T(8,128)(2,1)} %param.31) | copy-start | bytes 12582916
  112.3 18.4 %collective-permute-start.3 = (bf16[8,40,2048]{2,1,0:T(8,128)(2,1)}, bf16[8,40,2048]{2,1,0:T(8,128)(2,1)S(1)}, u32[]{:S(2)}, u32[]{:S(2)}) collective-permute-start(bf16[8,40,2048]{2,1,0:T(8,128)(2,1)} %collective-permute-done.2), channel_id=1, source_target_pairs={{0,1},{1,0},{2,3},{3,2},{4,5},{5,4},{6,7},{7,6},{8,9},{9,8},{10,11... | collective-permute-start | bytes 3932168 | tf_op jit(solution)/shard_map/ppermute | solution.py:203
  112.5 1.9 copy-start.10
  133.0 1.9 copy-start.14
  133.0 3.0 %copy-start.24 = (bf16[2,2048,512]{2,1,0:T(8,128)(2,1)S(1)}, bf16[2,2048,512]{2,1,0:T(8,128)(2,1)}, u32[]{:S(2)}) copy-start(bf16[2,2048,512]{2,1,0:T(8,128)(2,1)} %param.31) | copy-start | bytes 12582916
  143.6 1.4 copy-start.15
  154.2 1.4 copy-start.7
  154.2 1.4 copy-start.21
  154.2 1.4 copy-start.22
  154.2 3.0 %slice-start = ((bf16[384,2048]{1,0:T(8,128)(2,1)}), bf16[256,2048]{1,0:T(8,128)(2,1)S(1)}, s32[]{:S(2)}) async-start(bf16[384,2048]{1,0:T(8,128)(2,1)} %convolution_convert_fusion.2), calls=%async_computation.5 | async-start | bytes 2097152 | tf_op jit(solution)/shard_map/slice | solution.py:230
  157.5 1.6 copy-start.2
  159.1 1.8 copy-start.8
  159.1 2.9 %copy-start.16 = (bf16[512,256]{1,0:T(8,128)(2,1)S(1)}, bf16[512,256]{1,0:T(8,128)(2,1)}, u32[]{:S(2)}) copy-start(bf16[512,256]{1,0:T(8,128)(2,1)} %param.25) | copy-start | bytes 786436
  159.1 3.2 %copy-start.9 = (bf16[512,512]{1,0:T(8,128)(2,1)S(1)}, bf16[512,512]{1,0:T(8,128)(2,1)}, u32[]{:S(2)}) copy-start(bf16[512,512]{1,0:T(8,128)(2,1)} %get-tuple-element.28) | copy-start | bytes 1572868
  160.3 6.1 %collective-permute-start.4 = (bf16[8,40,2048]{2,1,0:T(8,128)(2,1)}, bf16[8,40,2048]{2,1,0:T(8,128)(2,1)}, u32[]{:S(2)}, u32[]{:S(2)}) collective-permute-start(bf16[8,40,2048]{2,1,0:T(8,128)(2,1)} %slice.209), channel_id=1, source_target_pairs={{0,1},{1,0},{2,3},{3,2},{4,5},{5,4},{6,7},{7,6},{8,9},{9,8},{10,11... | collective-permute-start | bytes 3932168 | tf_op jit(solution)/shard_map/ppermute | solution.py:203
  162.0 1.0 copy-start.12
  162.0 1.0 copy-start.20
  163.0 1.2 slice-start.1
  163.0 1.5 slice-start.2
  164.9 6.1 %copy-start.4 = (bf16[16,40,2048]{2,1,0:T(8,128)(2,1)}, bf16[16,40,2048]{2,1,0:T(8,128)(2,1)S(1)}, u32[]{:S(2)}) copy-start(bf16[16,40,2048]{2,1,0:T(8,128)(2,1)S(1)} %pad_maximum_fusion) | copy-start | bytes 7864324
  164.9 3.2 %copy-start.3 = (bf16[16,40,2048]{2,1,0:T(8,128)(2,1)S(1)}, bf16[16,40,2048]{2,1,0:T(8,128)(2,1)}, u32[]{:S(2)}) copy-start(bf16[16,40,2048]{2,1,0:T(8,128)(2,1)} %copy-done.2) | copy-start | bytes 7864324
  166.1 6.3 %slice-start.3 = ((bf16[512,256]{1,0:T(8,128)(2,1)}), bf16[512,128]{1,0:T(8,128)(2,1)S(1)}, s32[]{:S(2)}) async-start(bf16[512,256]{1,0:T(8,128)(2,1)} %param.24), calls=%async_computation.8 | async-start | bytes 262144 | tf_op jit(solution)/shard_map/slice | solution.py:160
  166.1 12.7 %collective-permute-start.1 = (bf16[8,40,2048]{2,1,0:T(8,128)(2,1)}, bf16[8,40,2048]{2,1,0:T(8,128)(2,1)}, u32[]{:S(2)}, u32[]{:S(2)}) collective-permute-start(bf16[8,40,2048]{2,1,0:T(8,128)(2,1)} %slice.200), channel_id=1, source_target_pairs={{0,1},{1,0},{2,3},{3,2},{4,5},{5,4},{6,7},{7,6},{8,9},{9,8},{10,11... | collective-permute-start | bytes 3932168 | tf_op jit(solution)/shard_map/ppermute | solution.py:203
  171.0 31.3 %collective-permute-start.5 = (bf16[8,40,2048]{2,1,0:T(8,128)(2,1)}, bf16[8,40,2048]{2,1,0:T(8,128)(2,1)}, u32[]{:S(2)}, u32[]{:S(2)}) collective-permute-start(bf16[8,40,2048]{2,1,0:T(8,128)(2,1)} %add_convert_fusion.1), channel_id=1, source_target_pairs={{0,2},{1,3},{2,0},{3,1},{4,6},{5,7},{6,4},{7,5},{8,10},{9,11},{10,... | collective-permute-start | bytes 3932168 | tf_op jit(solution)/shard_map/ppermute | solution.py:203
  172.4 2.5 copy-start.1
  206.2 3.7 %copy-start.19 = (f32[128,2]{0,1:T(2,128)S(1)}, f32[128,2]{0,1:T(2,128)}, u32[]{:S(2)}) copy-start(f32[128,2]{0,1:T(2,128)} %param.30) | copy-start | bytes 3076
  206.2 34.9 %all-to-all-start.1 = ((bf16[8,40,2048]{2,1,0:T(8,128)(2,1)}), bf16[8,40,2048]{2,1,0:T(8,128)(2,1)S(1)}, u32[]{:S(2)}, u32[]{:S(2)}) async-start(bf16[8,40,2048]{2,1,0:T(8,128)(2,1)} %add_convert_fusion), calls=%async_computation.2 | async-start | bytes 2621440 | tf_op jit(solution)/shard_map/all_to_all | solution.py:292
Sparse Core Ops, SparseCore 0:
  27.8 84.6 all-gather.1
  178.9 42.5 reduce-scatter.1
where the time goes:
time: 250 us
  waiting for transfers between devices  121 us (48%)
  matrix products  40 us (16%)
  local copies, waits for them, and re-layouts  27.1 us (11%)
  other arithmetic  18.7 us (7%)
  starting transfers between devices  14.8 us (6%)
  between operations  14.6 us (6%)
  blocking collectives  11.8 us (5%)
    ppermute x6, waiting for transfers between devices, swap(): return lax.ppermute(values, 'tp', [(one, one ^ bit) for one in range(size)])  55.2 us
    all_to_all x1, waiting for transfers between devices, experts_half(): lax.all_to_all(outgoing, 'ep', split_axis=0, concat_axis=0, tiled=True)  33.8 us
    all_to_all x1, waiting for transfers between devices, experts_half(): lax.all_to_all(summed, 'ep', split_axis=0, concat_axis=0, tiled=True)  31 us
    dot_general x4, matrix products, expert_rows(): jnp.dot(hidden, down_w[expert], preferred_element_type=jnp.float32)  23.4 us
    unnamed x54, local copies, waits for them, and re-layouts  12 us
    all_gather x1, blocking collectives, mixer_front(): lax.all_gather(rms_scale(query_latent, query_gain), 'tp', axis=0, tiled=T...  11.8 us
    dot_general x4, matrix products, expert_rows(): jnp.dot(inputs, gate_w[expert], preferred_element_type=jnp.float32)  9.08 us
    all_to_all x1, starting transfers between devices, experts_half(): lax.all_to_all(outgoing, 'ep', split_axis=0, concat_axis=0, tiled=True)  7.41 us
  transfers between devices with their start and end apart: 10, of which 4 were waited for; matrix products, arithmetic and copies ran while one was open for 27% of the time, Pallas kernels for 1%

commit v1 on v0

--- a/solution.py
+++ b/solution.py
@@ -302,7 +302,7 @@
     return (both[:tok_rows] + both[tok_rows:]).astype(jnp.bfloat16), latents
 
 
-def per_device(
+def plain_device(
     query_latent,
     kv_latent,
     rope_key,
@@ -337,6 +337,641 @@
     return (mixer_out, expert_out)
 
 
+MESH = pl.DeviceIdType.MESH
+
+
+def partner(index, bits):
+    place = 1
+    while place <= bits:
+        if bits & place:
+            index = index + place * (1 - 2 * ((index // place) % 2))
+        place *= 2
+    return index
+
+
+class Mail:
+    def __init__(self, ep, tp):
+        self.ep, self.tp, self.sent = ep, tp, []
+
+    def copy(self, source, target, sems, number, ep=0, tp=0, up=0):
+        return pltpu.make_async_remote_copy(
+            src_ref=source,
+            dst_ref=target,
+            send_sem=sems.at[0, number],
+            recv_sem=sems.at[1, number],
+            device_id=(partner(self.ep, ep) + up, partner(self.tp, tp)),
+            device_id_type=MESH,
+        )
+
+
+def expert_step(step, main, rest, recv, lhs, held, gate_w, up_w, down_w):
+    local = gate_w.shape[0]
+    depth = lhs.shape[1]
+    chunks = recv.shape[1] * 2
+    mains = chunks * main
+    rests = chunks * local * rest
+    span = slice(2 * step, 2 * step + 2)
+    tail = slice(local * main, local * (main + rest))
+    lhs[mains : mains + rests, :] = (
+        recv[span, :, tail, :].astype(jnp.float32).reshape(rests, depth).astype(jnp.bfloat16)
+    )
+    wide = 512
+
+    @pl.loop(0, 1)
+    def _(_unused):
+        for a in range(local):
+            own = slice(a * main, (a + 1) * main)
+            lhs[:mains, :] = recv[span, :, own, :].reshape(mains, depth)
+            gate = jnp.minimum(
+                jnp.dot(lhs[...], gate_w[a], preferred_element_type=jnp.float32), 7.0
+            )
+            upper = jnp.clip(
+                jnp.dot(lhs[...], up_w[a], preferred_element_type=jnp.float32), -7.0, 7.0
+            )
+            hidden = (gate * jax.nn.sigmoid(1.702 * gate) * (upper + 1.0)).astype(jnp.bfloat16)
+            for first in range(0, depth, wide):
+                cols = slice(first, first + wide)
+                out = jnp.dot(hidden, down_w[a, :, cols], preferred_element_type=jnp.float32)
+                recv[span, :, own, cols] = (
+                    out[:mains].astype(jnp.bfloat16).reshape(2, chunks // 2, main, wide)
+                )
+                if a == 0:
+                    held[:, cols] = out[mains:]
+                else:
+                    row = lax.broadcasted_iota(jnp.int32, (rests, wide), 0) % (local * rest)
+                    picked = jnp.where(row // rest == a, out[mains:], held[:, cols])
+                    if a < local - 1:
+                        held[:, cols] = picked
+                    else:
+                        recv[span, :, tail, cols] = picked.reshape(
+                            2, chunks // 2, local * rest, wide
+                        ).astype(jnp.bfloat16)
+
+
+def fused_kernel(
+    heads,
+    rope,
+    main,
+    rest,
+    outgoing,
+    lat_in,
+    q_in,
+    cos,
+    sin,
+    query_w,
+    key_w,
+    value_w,
+    output_w,
+    gate_h,
+    up_h,
+    down_h,
+    back,
+    mixed_out,
+    gate_w,
+    up_w,
+    down_w,
+    recv,
+    sibling,
+    chip,
+    far,
+    done,
+    lhs,
+    held,
+    lat,
+    queries,
+    heads_q,
+    peak,
+    total,
+    acc,
+    attended,
+    mixed,
+    mix_sib,
+    mix_chip,
+    mix_far,
+    load_sem,
+    go,
+    near_a,
+    near_b,
+    over,
+    part,
+    ret,
+    home,
+    lat_sem,
+    chain_up,
+    chain_sib,
+    chain_x,
+    chain_xs,
+    q_sem,
+    mix_sem,
+):
+    groups = outgoing.shape[0]
+    levels = groups // 2
+    steps = groups // 2
+    rows = lat_in.shape[0]
+    ep, tp = lax.axis_index("ep"), lax.axis_index("tp")
+    level, y, core = ep // 2, tp // 2, tp % 2
+    box = Mail(ep, tp)
+
+    loads = [
+        pltpu.make_async_copy(gate_h, gate_w, load_sem.at[0]),
+        pltpu.make_async_copy(up_h, up_w, load_sem.at[1]),
+        pltpu.make_async_copy(down_h, down_w, load_sem.at[2]),
+        pltpu.make_async_copy(outgoing.at[ep], recv.at[0, 0], load_sem.at[3]),
+        pltpu.make_async_copy(lat_in, lat.at[ep, y, core], load_sem.at[4]),
+        pltpu.make_async_copy(q_in, queries.at[y, core], load_sem.at[5]),
+    ]
+    for one in loads:
+        one.start()
+
+    barrier = pltpu.get_barrier_semaphore()
+    for bits in range(1, groups):
+        pl.semaphore_signal(
+            barrier, inc=1, device_id=(partner(ep, bits), tp), device_id_type=MESH
+        )
+    for bits in (1, 2):
+        pl.semaphore_signal(
+            barrier, inc=1, device_id=(ep, partner(tp, bits)), device_id_type=MESH
+        )
+    pl.semaphore_wait(barrier, groups + 1)
+
+    def dispatch(s):
+        return box.copy(outgoing.at[partner(ep, s)], recv.at[s, 0], go, s, ep=s)
+
+    def first(s):
+        return outgoing.at[ep] if s == 0 else recv.at[s, 0]
+
+    def to_over(s):
+        return box.copy(first(s), recv.at[s, 1], over, s, tp=2)
+
+    def to_near(s):
+        return box.copy(first(s), recv.at[s, 2], near_a, s, tp=1)
+
+    def to_near_over(s):
+        return box.copy(recv.at[s, 1], recv.at[s, 3], near_b, s, tp=1)
+
+    def to_part(k):
+        return box.copy(
+            recv.at[2 * k : 2 * k + 2, 2:4], sibling.at[2 * k : 2 * k + 2], part, k, tp=1
+        )
+
+    def to_far(s):
+        return box.copy(chip.at[s], far.at[s], ret, s, tp=2)
+
+    def to_home(s):
+        return box.copy(done.at[s], back.at[ep], home, s, ep=s)
+
+    def forward(s):
+        if s:
+            dispatch(s).wait_recv()
+        to_over(s).start()
+        to_near(s).start()
+
+    def cross(s):
+        to_over(s).wait_recv()
+        to_near_over(s).start()
+
+    def compute(k):
+        for s in (2 * k, 2 * k + 1):
+            to_near(s).wait_recv()
+            to_near_over(s).wait_recv()
+            to_over(s).wait_send()
+            to_near(s).wait_send()
+            to_near_over(s).wait_send()
+        expert_step(k, main, rest, recv, lhs, held, gate_w, up_w, down_w)
+        to_part(k).start()
+
+    def chip_sum(k):
+        to_part(k).wait_recv()
+        for s in (2 * k, 2 * k + 1):
+            chip[s] = add_rounded(recv[s, 1], sibling[s, 1])
+            to_far(s).start()
+            recv[s, 0] = add_rounded(recv[s, 0], sibling[s, 0])
+
+    def finish(k):
+        for s in (2 * k, 2 * k + 1):
+            to_far(s).wait_recv()
+            if s == 0:
+                back[ep] = add_rounded(recv[s, 0], far[s])
+            else:
+                done[s] = add_rounded(recv[s, 0], far[s])
+                to_home(s).start()
+
+    lat_over = box.copy(lat_in, lat.at[ep, y, core], lat_sem, 0, tp=2)
+    lat_near = box.copy(lat_in, lat.at[ep, y, core], lat_sem, 1, tp=1)
+    over_block = lat.at[ep, 1 - y, core]
+    lat_near_over = box.copy(over_block, over_block, lat_sem, 2, tp=1)
+    q_over = box.copy(q_in, queries.at[y, core], q_sem, 0, tp=2)
+    q_near = box.copy(q_in, queries.at[y, core], q_sem, 1, tp=1)
+    q_over_block = queries.at[1 - y, core]
+    q_near_over = box.copy(q_over_block, q_over_block, q_sem, 2, tp=1)
+
+    def blocks(group):
+        return lat.at[group, :, core]
+
+    def go_up(k):
+        own = blocks(ep - 2 * k)
+        return box.copy(own, own, chain_up, k, up=2)
+
+    def go_near(k):
+        own = blocks(ep - 2 * k)
+        return box.copy(own, own, chain_sib, k, tp=1)
+
+    def go_side(k):
+        own = blocks(ep - 2 * k)
+        return box.copy(own, own, chain_x, k, ep=1)
+
+    def go_side_near(k):
+        own = blocks(partner(ep, 1) - 2 * k)
+        return box.copy(own, own, chain_xs, k, tp=1)
+
+    def chain(k):
+        @pl.when(level >= k)
+        def _():
+            if k:
+                box.copy(blocks(ep - 2 * k), blocks(ep - 2 * k), chain_up, k - 1, up=2).wait_recv()
+                go_near(k).start()
+            if k < levels - 1:
+
+                @pl.when(level < levels - 1)
+                def _():
+                    go_up(k).start()
+
+            go_side(k).start()
+
+    def chain_side(k):
+        @pl.when(level >= k)
+        def _():
+            go_side(k).wait_recv()
+            go_side_near(k).start()
+
+    def chain_end(k):
+        @pl.when(level >= k)
+        def _():
+            if k:
+                go_near(k).wait_recv()
+                go_near(k).wait_send()
+            go_side_near(k).wait_recv()
+            go_side_near(k).wait_send()
+            go_side(k).wait_send()
+            if k < levels - 1:
+
+                @pl.when(level < levels - 1)
+                def _():
+                    go_up(k).wait_send()
+
+    def project_queries():
+        flat = jnp.dot(
+            queries[...].reshape(4 * rows, queries.shape[3]),
+            query_w[...],
+            preferred_element_type=jnp.float32,
+        )
+        nope_all = heads * NOPE
+        rope_all = heads * rope
+        rot = (
+            flat[:, nope_all : nope_all + rope_all] * cos[...]
+            + flat[:, nope_all + rope_all :] * sin[...]
+        )
+        lane = lax.broadcasted_iota(jnp.int32, rot.shape, 1)
+        for h in range(heads):
+            heads_q[:, h * PAD : h * PAD + NOPE] = flat[:, h * NOPE : (h + 1) * NOPE].astype(
+                jnp.bfloat16
+            )
+            heads_q[:, h * PAD + NOPE : (h + 1) * PAD] = jnp.where(
+                lane // rope == h, rot, 0.0
+            ).astype(jnp.bfloat16)
+
+    def attention():
+        count = 4 * rows
+        vdim = value_w.shape[0] // heads
+        scale = math.log2(math.e) / math.sqrt(NOPE + rope)
+        peak[...] = jnp.full_like(peak, -1e30)
+        total[...] = jnp.zeros_like(total)
+        acc[...] = jnp.zeros_like(acc)
+
+        def block(number, masked):
+            seen = lat[number].reshape(count, lat.shape[4])
+            keys = jnp.dot(seen, key_w[...], preferred_element_type=jnp.float32).astype(
+                jnp.bfloat16
+            )
+            vals = lax.dot_general(
+                value_w[...], seen, NT, preferred_element_type=jnp.float32
+            ).astype(jnp.bfloat16)
+            for h in range(heads):
+                score = (
+                    lax.dot_general(
+                        keys[:, h * PAD : (h + 1) * PAD],
+                        heads_q[:, h * PAD : (h + 1) * PAD],
+                        NT,
+                        preferred_element_type=jnp.float32,
+                    )
+                    * scale
+                )
+                if masked:
+                    key = lax.broadcasted_iota(jnp.int32, score.shape, 0)
+                    query = lax.broadcasted_iota(jnp.int32, score.shape, 1)
+                    score = jnp.where(key <= query, score, -1e30)
+                old = peak[h : h + 1, :]
+                new = jnp.maximum(old, jnp.max(score, axis=0, keepdims=True))
+                expo = jnp.exp2(score - new)
+                factor = jnp.exp2(old - new)
+                peak[h : h + 1, :] = new
+                total[h : h + 1, :] = total[h : h + 1, :] * factor + jnp.sum(
+                    expo, axis=0, keepdims=True
+                )
+                part_rows = slice(h * vdim, (h + 1) * vdim)
+                acc[part_rows, :] = acc[part_rows, :] * factor + jnp.dot(
+                    vals[part_rows, :], expo.astype(jnp.bfloat16), preferred_element_type=jnp.float32
+                )
+
+        @pl.loop(0, ep)
+        def _(number):
+            block(number, False)
+
+        block(ep, True)
+        for h in range(heads):
+            part_rows = slice(h * vdim, (h + 1) * vdim)
+            attended[:, part_rows] = (acc[part_rows, :] / total[h : h + 1, :]).T.astype(
+                jnp.bfloat16
+            )
+
+    def mix(owner_y, owner_core):
+        start = pl.multiple_of((owner_y * 2 + owner_core) * rows, rows)
+        return jnp.dot(
+            attended[pl.ds(start, rows), :], output_w[...], preferred_element_type=jnp.float32
+        ).astype(jnp.bfloat16)
+
+    mix_near = box.copy(mixed.at[2:4], mix_sib, mix_sem, 0, tp=1)
+    mix_over = box.copy(mix_chip, mix_far, mix_sem, 1, tp=2)
+
+    for s in range(1, groups):
+        dispatch(s).start()
+    forward(0)
+    lat_over.start()
+    lat_near.start()
+    forward(1)
+    cross(0)
+    lat_over.wait_recv()
+    lat_near_over.start()
+    loads[4].wait()
+    chain(0)
+    q_over.start()
+    q_near.start()
+    loads[0].wait()
+    loads[1].wait()
+    loads[2].wait()
+    loads[3].wait()
+    loads[5].wait()
+    for s in (2, 3):
+        forward(s)
+    cross(1)
+    for k in range(steps):
+        compute(k)
+        for s in (2 * k + 2, 2 * k + 3):
+            if s < groups:
+                cross(s)
+        for s in (2 * k + 4, 2 * k + 5):
+            if s < groups:
+                forward(s)
+        if k == 0:
+            q_over.wait_recv()
+            q_near_over.start()
+            chain_side(0)
+        if k:
+            chain(k)
+        chip_sum(k)
+        if k:
+            finish(k - 1)
+            chain_side(k)
+    for k in range(steps, levels):
+        chain(k)
+        chain_side(k)
+    finish(steps - 1)
+    q_near.wait_recv()
+    q_near_over.wait_recv()
+    project_queries()
+    lat_near.wait_recv()
+    lat_near_over.wait_recv()
+    for k in range(levels):
+        chain_end(k)
+    attention()
+    mixed[2] = mix(y, 1 - core)
+    mixed[3] = mix(1 - y, 1 - core)
+    mix_near.start()
+    mixed[0] = mix(y, core)
+    mixed[1] = mix(1 - y, core)
+    mix_near.wait_recv()
+    mix_chip[...] = add_rounded(mixed[1], mix_sib[1])
+    mix_over.start()
+    mixed[0] = add_rounded(mixed[0], mix_sib[0])
+    mix_over.wait_recv()
+    mixed_out[...] = add_rounded(mixed[0], mix_far[...])
+    for s in range(1, groups):
+        to_home(s).wait_recv()
+    for s in range(1, groups):
+        dispatch(s).wait_send()
+        to_home(s).wait_send()
+    for s in range(groups):
+        to_far(s).wait_send()
+    for k in range(steps):
+        to_part(k).wait_send()
+    for one in (lat_over, lat_near, lat_near_over, q_over, q_near, q_near_over, mix_near, mix_over):
+        one.wait_send()
+
+
+def fused(
+    outgoing, lat, query, cos, sin, query_w, key_w, value_w, output_w, gate_w, up_w, down_w, sizes
+):
+    heads, rope, main, rest = sizes
+    groups, piece, depth = outgoing.shape
+    rows, lat_width = lat.shape
+    local = gate_w.shape[0]
+    pair = (2, piece, depth)
+    chunks = 8
+    mains = chunks * main
+    rests = chunks * local * rest
+    bf, fl = jnp.bfloat16, jnp.float32
+    vmem = pl.BlockSpec(memory_space=pltpu.VMEM)
+    hbm = pl.BlockSpec(memory_space=pl.ANY)
+    levels = groups // 2
+    sem = pltpu.SemaphoreType.DMA
+    scratch = [
+        pltpu.VMEM(gate_w.shape, bf),
+        pltpu.VMEM(up_w.shape, bf),
+        pltpu.VMEM(down_w.shape, bf),
+        pltpu.VMEM((groups, 4, piece, depth), bf),
+        pltpu.VMEM((groups,) + pair, bf),
+        pltpu.VMEM((groups, piece, depth), bf),
+        pltpu.VMEM((groups, piece, depth), bf),
+        pltpu.VMEM((groups, piece, depth), bf),
+        pltpu.VMEM((mains + rests, depth), bf),
+        pltpu.VMEM((rests, depth), fl),
+        pltpu.VMEM((groups, 2, 2, rows, lat_width), bf),
+        pltpu.VMEM((2, 2) + query.shape, bf),
+        pltpu.VMEM((4 * rows, heads * PAD), bf),
+        pltpu.VMEM((heads, 4 * rows), fl),
+        pltpu.VMEM((heads, 4 * rows), fl),
+        pltpu.VMEM((value_w.shape[0], 4 * rows), fl),
+        pltpu.VMEM((4 * rows, value_w.shape[0]), bf),
+        pltpu.VMEM((4, rows, depth), bf),
+        pltpu.VMEM((2, rows, depth), bf),
+        pltpu.VMEM((rows, depth), bf),
+        pltpu.VMEM((rows, depth), bf),
+        sem((6,)),
+        sem((2, groups)),
+        sem((2, groups)),
+        sem((2, groups)),
+        sem((2, groups)),
+        sem((2, groups // 2)),
+        sem((2, groups)),
+        sem((2, groups)),
+        sem((2, 3)),
+        sem((2, levels)),
+        sem((2, levels)),
+        sem((2, levels)),
+        sem((2, levels)),
+        sem((2, 3)),
+        sem((2, 2)),
+    ]
+    return pl.pallas_call(
+        functools.partial(fused_kernel, heads, rope, main, rest),
+        out_shape=(
+            jax.ShapeDtypeStruct(outgoing.shape, bf),
+            jax.ShapeDtypeStruct((rows, depth), bf),
+        ),
+        in_specs=[vmem] * 9 + [hbm] * 3,
+        out_specs=(vmem, vmem),
+        scratch_shapes=scratch,
+        compiler_params=pltpu.CompilerParams(
+            collective_id=0, has_side_effects=True, vmem_limit_bytes=60 * 1024 * 1024
+        ),
+    )(outgoing, lat, query, cos, sin, query_w, key_w, value_w, output_w, gate_w, up_w, down_w)
+
+
+def per_device(
+    query_latent,
+    kv_latent,
+    rope_key,
+    query_gain,
+    kv_gain,
+    query_nope_w,
+    query_rope_w,
+    key_up_w,
+    value_up_w,
+    output_w,
+    expert_in,
+    moe_gain,
+    routes,
+    route_weight,
+    gate_w,
+    up_w,
+    down_w,
+):
+    tok_rows, top_count = routes.shape
+    width = expert_in.shape[1]
+    local = gate_w.shape[0]
+    rope = rope_key.shape[1]
+    heads = query_nope_w.shape[1] // NOPE
+    ep_size, tp_size = lax.axis_size("ep"), lax.axis_size("tp")
+    experts = local * ep_size
+    capacity = max(2, 5 * tok_rows * top_count // (4 * experts))
+    main = capacity // 8 * 8
+    rest = capacity - main
+    if not (
+        tp_size == 4
+        and ep_size & (ep_size - 1) == 0
+        and main % 16 == 0
+        and local * rest % 8 == 0
+        and heads * rope == 128
+    ):
+        return plain_device(
+            query_latent,
+            kv_latent,
+            rope_key,
+            query_gain,
+            kv_gain,
+            query_nope_w,
+            query_rope_w,
+            key_up_w,
+            value_up_w,
+            output_w,
+            expert_in,
+            moe_gain,
+            routes,
+            route_weight,
+            gate_w,
+            up_w,
+            down_w,
+        )
+    half = rope // 2
+    group_rows = tok_rows * tp_size
+    freq = 1.0 / THETA ** (jnp.arange(half, dtype=jnp.float32) * 2.0 / rope)
+    first_pos = lax.axis_index("ep") * group_rows
+    positions = first_pos + jnp.arange(group_rows, dtype=jnp.int32)
+    own = lax.axis_index("tp") * tok_rows + first_pos + jnp.arange(tok_rows, dtype=jnp.int32)
+    own_angle = own.astype(jnp.float32)[:, None] * jnp.tile(freq, 2)[None, :]
+    keys = rope_key.astype(jnp.float32)
+    turned = jnp.concatenate([-keys[:, half:], keys[:, :half]], axis=-1)
+    key_rot = (keys * jnp.cos(own_angle) + turned * jnp.sin(own_angle)).astype(jnp.bfloat16)
+    own_latents = jnp.concatenate([rms_scale(kv_latent, kv_gain), key_rot], axis=1)
+    own_query = rms_scale(query_latent, query_gain)
+    angle = positions.astype(jnp.float32)[:, None] * jnp.tile(freq, 2 * heads)[None, :]
+    turned_w = []
+    for h in range(heads):
+        turned_w.append(-query_rope_w[:, h * rope + half : (h + 1) * rope])
+        turned_w.append(query_rope_w[:, h * rope : h * rope + half])
+    query_w = jnp.concatenate([query_nope_w, query_rope_w] + turned_w, axis=1)
+    key_w = jnp.concatenate(
+        [
+            jnp.concatenate(
+                [
+                    jnp.pad(key_up_w[:, h * NOPE : (h + 1) * NOPE], ((0, 0), (0, PAD - NOPE))),
+                    jnp.pad(
+                        jnp.eye(rope, dtype=jnp.bfloat16),
+                        ((0, 0), (NOPE + h * rope, PAD - NOPE - (h + 1) * rope)),
+                    ),
+                ],
+                axis=0,
+            )
+            for h in range(heads)
+        ],
+        axis=1,
+    )
+    value_w = jnp.pad(value_up_w.T, ((0, 0), (0, rope)))
+    floats = expert_in.astype(jnp.float32)
+    center = floats - jnp.mean(floats, axis=-1, keepdims=True)
+    variance = jnp.mean(center * center, axis=-1, keepdims=True)
+    normed_in = (center * lax.rsqrt(variance + 1e-05) * moe_gain).astype(jnp.bfloat16)
+    hits = route(routes, experts, local, capacity)
+    select = functools.reduce(jnp.logical_or, hits).astype(jnp.bfloat16)
+    outgoing = (
+        lax.dot_general(select, normed_in, (((0,), (0,)), ((), ())), preferred_element_type=jnp.float32)
+        .astype(jnp.bfloat16)
+        .reshape(ep_size, local * capacity, width)
+    )
+    back, mixer_out = fused(
+        outgoing,
+        own_latents,
+        own_query,
+        jnp.cos(angle),
+        jnp.sin(angle),
+        query_w,
+        key_w,
+        value_w,
+        output_w,
+        gate_w,
+        up_w,
+        down_w,
+        (heads, rope, main, rest),
+    )
+    back = back.reshape(experts * capacity, width)
+    weights = route_weight / jnp.sum(route_weight, axis=-1, keepdims=True)
+    mix = sum(jnp.where(hit, weights[:, k : k + 1], 0.0) for k, hit in enumerate(hits))
+    high = mix.astype(jnp.bfloat16)
+    low = (mix - high.astype(jnp.float32)).astype(jnp.bfloat16)
+    both = jnp.dot(jnp.concatenate([high, low], axis=0), back, preferred_element_type=jnp.float32)
+    return mixer_out, (both[:tok_rows] + both[tok_rows:]).astype(jnp.bfloat16)
+
+
 def solution(mesh):
     placed = (
         P(("ep", "tp"), None),

time: 250 us -> 126 us (0.50)
  the two profiles are of different devices: /device:TPU:0 before, /device:TPU:31 now
where the time goes in v1:
time: 126 us
  Pallas kernels  107 us (85%)
  other arithmetic  8.86 us (7%)
  local copies, waits for them, and re-layouts  4.79 us (4%)
  matrix products  4.66 us (4%)
    pallas_call x1, Pallas kernels, fused(): pl.pallas_call(functools.partial(fused_kernel, heads, rope, main, rest),...  107 us

profile of v1, /device:TPU:31, one launch (start us, length us, event | category | flops | bytes accessed | tf_op | source)
XLA Modules:
  0.0 126.0 jit_solution(1297957164688485439)
XLA Ops:
  0.6 0.0 copy-start.1
  0.6 0.8 slice_bitcast_fusion.3
  1.4 0.2 select_reduce_fusion.1
  1.6 1.2 convert_reduce_fusion
  2.8 1.4 %fusion.11 = f32[128]{0:T(128)S(1)} fusion(bf16[128,2048]{1,0:T(8,128)(2,1)} %param.27, f32[128]{0:T(128)S(1)} %broadcast_multiply_fusion), kind=kLoop, calls=%fused_computation.19 | loop fusion | flops 1048448 | bytes 525312 | tf_op jit(solution)/shard_map/reduce_sum | solution.py:942
  4.2 0.0 copy-done.1
  4.2 0.0 copy-start.6
  4.2 2.5 %convolution_convert_fusion = bf16[320,2048]{1,0:T(8,128)(2,1)} fusion(bf16[128,2048]{1,0:T(8,128)(2,1)S(1)} %copy-done.1, f32[2048]{0:T(1024)} %param.28, f32[128]{0:T(128)S(1)} %add_rsqrt_fusion.2, f32[128]{0:T(128)S(1)} %broadcast_multiply_fusion, s32[128]{0:T(128)S(1)} %get-tuple-element.7, s32[128]{0:T(128)S(1)} %get-tuple-element.6), kind=kOutput, calls=%fused_computation | convolution fusion | flops 169861120 | bytes 1845248 | tf_op jit(solution)/shard_map/dot_general | solution.py:947
  6.7 0.0 copy-done
  6.7 0.2 fusion.50
  6.9 0.0 copy-start.8
  6.9 0.0 copy-done.6
  6.9 0.0 copy-start.5
  6.9 0.0 copy-start.11
  6.9 1.8 %concatenate.23.query_w = bf16[768,512]{1,0:T(8,128)(2,1)} concatenate(bf16[768,256]{1,0:T(8,128)(2,1)S(1)} %copy-done.6, bf16[768,128]{1,0:T(8,128)(2,1)S(1)} %copy-done, bf16[768,32]{1,0:T(8,128)(2,1)S(1)} %get-tuple-element.11, bf16[768,32]{1,0:T(8,128)(2,1)S(1)} %get-tuple-element.10, bf16[768,32]{1,0:T(8,128)(2,1)S(1)} %get-tuple-element.9, bf16[768,32]{1,0:T(8,128)(2,1)S(1)} %get-tuple-element.8), dimensions={1} | concatenate | bytes 1572864 | tf_op jit(solution)/shard_map/concatenate | solution.py:922
  8.8 0.0 copy-done.8
  8.8 0.1 copy.19
  8.9 0.0 slice-start
  8.9 0.1 slice_negate_fusion.2
  9.0 0.1 mul.142
  9.1 0.3 fusion.39
  9.4 0.0 copy-done.5
  9.5 0.1 fusion.25
  9.6 0.0 copy-done.11
  9.6 0.1 fusion.27
  9.7 0.0 copy-start.7
  9.7 0.7 pad_maximum_fusion.lat_in
  10.4 0.1 mul.153
  10.5 1.8 %multiply_sine_fusion = (f32[512,128]{1,0:T(8,128)}, f32[512,128]{1,0:T(8,128)}) fusion(f32[128]{0:T(128)S(1)} %mul.153, f32[512]{0:T(512)S(1)} %add_convert_fusion), kind=kLoop, calls=%fused_computation.35 | loop fusion | flops 65536 | bytes 526848 | tf_op jit(solution)/shard_map/sin | solution.py:956
  12.3 0.0 copy-done.3
  12.3 0.0 copy-done.12
  12.3 0.0 copy-start.2
  12.3 0.0 copy-start.9
  12.4 0.0 slice-done
  12.4 0.9 fusion.16.key_w
  13.3 0.0 copy-done.7
  13.3 0.1 copy.20
  13.4 0.8 pad.23.value_w
  14.2 0.0 copy-done.2
  14.2 0.1 fusion.22
  14.3 0.0 copy-done.9
  14.3 0.8 fusion.24.q_in
  15.1 106.8 %shard_map.176 = (bf16[8,40,2048]{2,1,0:T(8,128)(2,1)}, bf16[128,2048]{1,0:T(8,128)(2,1)}) custom-call(bf16[8,40,2048]{2,1,0:T(8,128)(2,1)} %bitcast.12, bf16[128,576]{1,0:T(8,128)(2,1)} %pad_maximum_fusion.lat_in, bf16[128,768]{1,0:T(8,128)(2,1)} %fusion.24.q_in, f32[512,128]{1,0:T(8,128)} %get-tuple-element.13.cos, f32[512,128]{1,0:T(8,128)} %get-tuple-element.12.sin, ...), custom_call_target="tpu_custom_call" | custom-call | tf_op jit(solution)/shard_map/pallas_call | solution.py:835
  122.0 0.1 fusion.32
  122.1 2.0 %fusion.28 = f32[256,2048]{1,0:T(8,128)S(1)} fusion(bf16[320,2048]{1,0:T(8,128)(2,1)} %bitcast.13, bf16[128,320]{1,0:T(8,128)(2,1)S(1)} %get-tuple-element.15, bf16[128,320]{1,0:T(8,128)(2,1)S(1)} %get-tuple-element.14), kind=kOutput, calls=%fused_computation.43 | convolution fusion | flops 335872000 | bytes 3571712 | tf_op jit(solution)/shard_map/dot_general | solution.py:971
  124.2 0.9 fusion.14
  125.1 0.2 copy-done.4
  125.2 0.8 copy.22
  (24 shorter events, 0.1 us)
Async XLA Ops:
  0.6 3.5 %copy-start.1 = (bf16[128,2048]{1,0:T(8,128)(2,1)S(1)}, bf16[128,2048]{1,0:T(8,128)(2,1)}, u32[]{:S(2)}) copy-start(bf16[128,2048]{1,0:T(8,128)(2,1)} %param.27) | copy-start | bytes 1572868
  2.8 3.9 %copy-start = (bf16[768,128]{1,0:T(8,128)(2,1)S(1)}, bf16[768,128]{1,0:T(8,128)(2,1)}, u32[]{:S(2)}) copy-start(bf16[768,128]{1,0:T(8,128)(2,1)} %param.23) | copy-start | bytes 589828
  4.2 2.7 %copy-start.6 = (bf16[768,256]{1,0:T(8,128)(2,1)S(1)}, bf16[768,256]{1,0:T(8,128)(2,1)}, u32[]{:S(2)}) copy-start(bf16[768,256]{1,0:T(8,128)(2,1)} %param.22) | copy-start | bytes 1179652
  6.9 1.9 %copy-start.8 = (bf16[128,64]{0,1:T(8,128)(2,1)S(1)}, bf16[128,64]{0,1:T(8,128)(2,1)}, u32[]{:S(2)}) copy-start(bf16[128,64]{0,1:T(8,128)(2,1)} %param.19) | copy-start | bytes 49156
  6.9 2.5 %copy-start.5 = (bf16[128,512]{1,0:T(8,128)(2,1)S(1)}, bf16[128,512]{1,0:T(8,128)(2,1)}, u32[]{:S(2)}) copy-start(bf16[128,512]{1,0:T(8,128)(2,1)} %param.18) | copy-start | bytes 393220
  6.9 2.7 %copy-start.11 = (f32[512]{0:T(512)S(1)}, f32[512]{0:T(512)}, u32[]{:S(2)}) copy-start(f32[512]{0:T(512)} %param.21) | copy-start | bytes 6148
  8.7 3.5 %copy-start.3 = (bf16[512,256]{1,0:T(8,128)(2,1)S(1)}, bf16[512,256]{1,0:T(8,128)(2,1)}, u32[]{:S(2)}) copy-start(bf16[512,256]{1,0:T(8,128)(2,1)} %param.24) | copy-start | bytes 786436
  8.8 3.5 %copy-start.12 = (pred[256]{0:T(512)(128)(4,1)S(1)}, pred[256]{0:T(512)(128)(4,1)}, u32[]{:S(2)}) copy-start(pred[256]{0:T(512)(128)(4,1)} %constant.80.clone.1) | copy-start | bytes 772
  8.9 3.5 %slice-start = ((bf16[512,256]{1,0:T(8,128)(2,1)}), bf16[512,128]{1,0:T(8,128)(2,1)S(1)}, s32[]{:S(2)}) async-start(bf16[512,256]{1,0:T(8,128)(2,1)} %param.24), calls=%async_computation | async-start | bytes 262144 | tf_op jit(solution)/shard_map/slice | solution.py:927
  9.7 3.6 %copy-start.7 = (bf16[512,256]{1,0:T(8,128)(2,1)S(1)}, bf16[512,256]{1,0:T(8,128)(2,1)}, u32[]{:S(2)}) copy-start(bf16[512,256]{1,0:T(8,128)(2,1)} %param.25) | copy-start | bytes 786436
  12.3 1.9 %copy-start.2 = (bf16[128,768]{1,0:T(8,128)(2,1)S(1)}, bf16[128,768]{1,0:T(8,128)(2,1)}, u32[]{:S(2)}) copy-start(bf16[128,768]{1,0:T(8,128)(2,1)} %param.17) | copy-start | bytes 589828
  12.3 2.0 %copy-start.9 = (f32[768]{0:T(1024)S(1)}, f32[768]{0:T(1024)}, u32[]{:S(2)}) copy-start(f32[768]{0:T(1024)} %param.20) | copy-start | bytes 9220
  15.1 106.8 %copy-start.10 = (f32[128,2]{0,1:T(2,128)S(1)}, f32[128,2]{0,1:T(2,128)}, u32[]{:S(2)}) copy-start(f32[128,2]{0,1:T(2,128)} %param.30) | copy-start | bytes 3076
  124.1 1.1 copy-start.4

commit v2 on v1

--- a/solution.py
+++ b/solution.py
@@ -3,6 +3,7 @@
 
 import jax
 import jax.numpy as jnp
+import numpy as np
 from jax import lax
 from jax.experimental import pallas as pl
 from jax.experimental.pallas import tpu as pltpu
@@ -349,6 +350,17 @@
     return index
 
 
+def scoped(name):
+    def wrap(inner):
+        def run(*args):
+            with jax.named_scope(name + "".join(str(a) for a in args if isinstance(a, int))):
+                return inner(*args)
+
+        return run
+
+    return wrap
+
+
 class Mail:
     def __init__(self, ep, tp):
         self.ep, self.tp, self.sent = ep, tp, []
@@ -377,8 +389,7 @@
     )
     wide = 512
 
-    @pl.loop(0, 1)
-    def _(_unused):
+    if True:
         for a in range(local):
             own = slice(a * main, (a + 1) * main)
             lhs[:mains, :] = recv[span, :, own, :].reshape(mains, depth)
@@ -408,25 +419,86 @@
                         ).astype(jnp.bfloat16)
 
 
+def prepare_rows(local, main, rest, rows_in, moe_gain, routes, route_weight, outgoing, shares):
+    groups, piece, depth = outgoing.shape
+    rows = rows_in.shape[0]
+    experts = groups * local
+    floats = rows_in[...].astype(jnp.float32)
+    center = floats - jnp.mean(floats, axis=-1, keepdims=True)
+    variance = jnp.mean(center * center, axis=-1, keepdims=True)
+    normed = (center * lax.rsqrt(variance + 1e-05) * moe_gain[...][None, :]).astype(jnp.bfloat16)
+    chosen = [routes[k : k + 1, :] for k in range(routes.shape[0])]
+    names = lax.broadcasted_iota(jnp.int32, (experts, rows), 0)
+    match = [one == names for one in chosen]
+    member = jnp.where(functools.reduce(jnp.logical_or, match), 1.0, 0.0).astype(jnp.bfloat16)
+    before = lax.broadcasted_iota(jnp.int32, (rows, rows), 0) < lax.broadcasted_iota(
+        jnp.int32, (rows, rows), 1
+    )
+    rank = jnp.dot(
+        member, jnp.where(before, 1.0, 0.0).astype(jnp.bfloat16), preferred_element_type=jnp.float32
+    )
+    inner = (names % local).astype(jnp.float32)
+    start = ((names // local) * piece).astype(jnp.float32)
+    place = start + jnp.where(
+        rank < main, inner * main + rank, local * main + inner * rest + rank - main
+    )
+    places = [
+        jnp.sum(jnp.where(one, place, 0.0), axis=0, keepdims=True).astype(jnp.int32)
+        for one in match
+    ]
+    slots = lax.broadcasted_iota(jnp.int32, (groups * piece, rows), 0)
+    hits = [one == slots for one in places]
+    select = jnp.where(functools.reduce(jnp.logical_or, hits), 1.0, 0.0).astype(jnp.bfloat16)
+    outgoing[...] = (
+        jnp.dot(select, normed, preferred_element_type=jnp.float32)
+        .reshape(groups, piece, depth)
+        .astype(jnp.bfloat16)
+    )
+    loads = [route_weight[k : k + 1, :] for k in range(routes.shape[0])]
+    whole = sum(loads)
+    share = sum(jnp.where(hit, one / whole, 0.0) for hit, one in zip(hits, loads))
+    high = share.astype(jnp.bfloat16).astype(jnp.float32)
+    shares[:, :, :rows] = high.reshape(groups, piece, rows).astype(jnp.bfloat16)
+    shares[:, :, rows:] = (share - high).reshape(groups, piece, rows).astype(jnp.bfloat16)
+
+
 def fused_kernel(
     heads,
     rope,
     main,
     rest,
+    query_in,
+    kv_in,
+    rope_in,
+    query_gain,
+    kv_gain,
+    freq,
+    moe_gain,
+    routes,
+    route_weight,
+    rows_h,
+    nope_h,
+    rope_h,
+    key_h,
+    value_h,
+    output_h,
+    gate_h,
+    up_h,
+    down_h,
+    mixed_out,
+    expert_out,
+    rows_in,
     outgoing,
-    lat_in,
-    q_in,
-    cos,
-    sin,
-    query_w,
+    back,
+    shares,
+    blend,
+    nope_w,
+    rope_w,
     key_w,
     value_w,
     output_w,
-    gate_h,
-    up_h,
-    down_h,
-    back,
-    mixed_out,
+    value_t,
+    keys_s,
     gate_w,
     up_w,
     down_w,
@@ -438,6 +510,7 @@
     lhs,
     held,
     lat,
+    wide_key,
     queries,
     heads_q,
     peak,
@@ -465,10 +538,13 @@
     mix_sem,
 ):
     groups = outgoing.shape[0]
+    local = gate_w.shape[0]
     levels = groups // 2
     steps = groups // 2
-    rows = lat_in.shape[0]
+    rows = kv_in.shape[0]
+    kv_width = kv_in.shape[1]
     ep, tp = lax.axis_index("ep"), lax.axis_index("tp")
+    half = rope // 2
     level, y, core = ep // 2, tp // 2, tp % 2
     box = Mail(ep, tp)
 
@@ -476,11 +552,14 @@
         pltpu.make_async_copy(gate_h, gate_w, load_sem.at[0]),
         pltpu.make_async_copy(up_h, up_w, load_sem.at[1]),
         pltpu.make_async_copy(down_h, down_w, load_sem.at[2]),
-        pltpu.make_async_copy(outgoing.at[ep], recv.at[0, 0], load_sem.at[3]),
-        pltpu.make_async_copy(lat_in, lat.at[ep, y, core], load_sem.at[4]),
-        pltpu.make_async_copy(q_in, queries.at[y, core], load_sem.at[5]),
+        pltpu.make_async_copy(rows_h, rows_in, load_sem.at[3]),
+        pltpu.make_async_copy(nope_h, nope_w, load_sem.at[4]),
+        pltpu.make_async_copy(rope_h, rope_w, load_sem.at[5]),
+        pltpu.make_async_copy(key_h, key_w, load_sem.at[6]),
+        pltpu.make_async_copy(value_h, value_w, load_sem.at[7]),
+        pltpu.make_async_copy(output_h, output_w, load_sem.at[8]),
     ]
-    for one in loads:
+    for one in loads[3:] + loads[:3]:
         one.start()
 
     barrier = pltpu.get_barrier_semaphore()
@@ -492,7 +571,33 @@
         pl.semaphore_signal(
             barrier, inc=1, device_id=(ep, partner(tp, bits)), device_id_type=MESH
         )
-    pl.semaphore_wait(barrier, groups + 1)
+    lane = lax.broadcasted_iota(jnp.int32, (rows, 128), 1)
+    place = lax.broadcasted_iota(jnp.int32, (rows, 128), 0) + lane // half * rows
+    angle = (place + ep * (4 * rows)).astype(jnp.float32) * freq[...]
+    cos_all, sin_all = jnp.cos(angle), jnp.sin(angle)
+
+    def spread(table, block):
+        own = jnp.where(lane // half == block, table, 0.0)
+        own = own + pltpu.roll(own, half, 1)
+        return own + pltpu.roll(own, 2 * half, 1)
+
+    def rotate(values, block):
+        turned = jnp.where(
+            lane % rope < half, -pltpu.roll(values, 128 - half, 1), pltpu.roll(values, half, 1)
+        )
+        return values * spread(cos_all, block) + turned * spread(sin_all, block)
+
+    scope = jax.named_scope("latents")
+    scope.__enter__()
+    lat[ep, y, core, :, :kv_width] = rms_scale(kv_in[...], kv_gain[...][None, :])
+    raw_key = rope_in[...].astype(jnp.float32).T
+    wide_key[:, :rope] = raw_key
+    wide_key[:, rope:] = raw_key
+    lat[ep, y, core, :, kv_width:] = rotate(wide_key[...], tp)[:, :rope].astype(jnp.bfloat16)
+    queries[y, core] = rms_scale(query_in[...], query_gain[...][None, :])
+    scope.__exit__(None, None, None)
+    with jax.named_scope("barrier"):
+        pl.semaphore_wait(barrier, groups + 1)
 
     def dispatch(s):
         return box.copy(outgoing.at[partner(ep, s)], recv.at[s, 0], go, s, ep=s)
@@ -520,16 +625,19 @@
     def to_home(s):
         return box.copy(done.at[s], back.at[ep], home, s, ep=s)
 
+    @scoped("forward")
     def forward(s):
         if s:
             dispatch(s).wait_recv()
         to_over(s).start()
         to_near(s).start()
 
+    @scoped("cross")
     def cross(s):
         to_over(s).wait_recv()
         to_near_over(s).start()
 
+    @scoped("compute")
     def compute(k):
         for s in (2 * k, 2 * k + 1):
             to_near(s).wait_recv()
@@ -537,16 +645,20 @@
             to_over(s).wait_send()
             to_near(s).wait_send()
             to_near_over(s).wait_send()
-        expert_step(k, main, rest, recv, lhs, held, gate_w, up_w, down_w)
+        with jax.named_scope(f"expert{k}"):
+            expert_step(k, main, rest, recv, lhs, held, gate_w, up_w, down_w)
         to_part(k).start()
 
+    @scoped("chip_sum")
     def chip_sum(k):
         to_part(k).wait_recv()
         for s in (2 * k, 2 * k + 1):
             chip[s] = add_rounded(recv[s, 1], sibling[s, 1])
-            to_far(s).start()
+            if k >= groups // 4:
+                to_far(s).start()
             recv[s, 0] = add_rounded(recv[s, 0], sibling[s, 0])
 
+    @scoped("finish")
     def finish(k):
         for s in (2 * k, 2 * k + 1):
             to_far(s).wait_recv()
@@ -556,12 +668,13 @@
                 done[s] = add_rounded(recv[s, 0], far[s])
                 to_home(s).start()
 
-    lat_over = box.copy(lat_in, lat.at[ep, y, core], lat_sem, 0, tp=2)
-    lat_near = box.copy(lat_in, lat.at[ep, y, core], lat_sem, 1, tp=1)
+    own_block, own_query = lat.at[ep, y, core], queries.at[y, core]
+    lat_over = box.copy(own_block, own_block, lat_sem, 0, tp=2)
+    lat_near = box.copy(own_block, own_block, lat_sem, 1, tp=1)
     over_block = lat.at[ep, 1 - y, core]
     lat_near_over = box.copy(over_block, over_block, lat_sem, 2, tp=1)
-    q_over = box.copy(q_in, queries.at[y, core], q_sem, 0, tp=2)
-    q_near = box.copy(q_in, queries.at[y, core], q_sem, 1, tp=1)
+    q_over = box.copy(own_query, own_query, q_sem, 0, tp=2)
+    q_near = box.copy(own_query, own_query, q_sem, 1, tp=1)
     q_over_block = queries.at[1 - y, core]
     q_near_over = box.copy(q_over_block, q_over_block, q_sem, 2, tp=1)
 
@@ -584,6 +697,7 @@
         own = blocks(partner(ep, 1) - 2 * k)
         return box.copy(own, own, chain_xs, k, tp=1)
 
+    @scoped("chain")
     def chain(k):
         @pl.when(level >= k)
         def _():
@@ -598,12 +712,14 @@
 
             go_side(k).start()
 
+    @scoped("chain_side")
     def chain_side(k):
         @pl.when(level >= k)
         def _():
             go_side(k).wait_recv()
             go_side_near(k).start()
 
+    @scoped("chain_end")
     def chain_end(k):
         @pl.when(level >= k)
         def _():
@@ -619,81 +735,118 @@
                 def _():
                     go_up(k).wait_send()
 
+    @scoped("project_queries")
     def project_queries():
-        flat = jnp.dot(
-            queries[...].reshape(4 * rows, queries.shape[3]),
-            query_w[...],
-            preferred_element_type=jnp.float32,
-        )
-        nope_all = heads * NOPE
-        rope_all = heads * rope
-        rot = (
-            flat[:, nope_all : nope_all + rope_all] * cos[...]
-            + flat[:, nope_all + rope_all :] * sin[...]
-        )
-        lane = lax.broadcasted_iota(jnp.int32, rot.shape, 1)
-        for h in range(heads):
-            heads_q[:, h * PAD : h * PAD + NOPE] = flat[:, h * NOPE : (h + 1) * NOPE].astype(
-                jnp.bfloat16
-            )
-            heads_q[:, h * PAD + NOPE : (h + 1) * PAD] = jnp.where(
-                lane // rope == h, rot, 0.0
-            ).astype(jnp.bfloat16)
-
-    def attention():
-        count = 4 * rows
-        vdim = value_w.shape[0] // heads
-        scale = math.log2(math.e) / math.sqrt(NOPE + rope)
+        for block in range(4):
+            source = queries[block // 2, block % 2]
+            span = slice(block * rows, (block + 1) * rows)
+            flat = jnp.dot(source, nope_w[...], preferred_element_type=jnp.float32)
+            rot = rotate(
+                jnp.dot(source, rope_w[...], preferred_element_type=jnp.float32), block
+            )
+            for h in range(heads):
+                heads_q[span, h * PAD : h * PAD + NOPE] = flat[
+                    :, h * NOPE : (h + 1) * NOPE
+                ].astype(jnp.bfloat16)
+                shifted = pltpu.roll(rot, 128 - h * rope, 1) if h else rot
+                heads_q[span, h * PAD + NOPE : (h + 1) * PAD] = jnp.where(
+                    lane < rope, shifted, 0.0
+                ).astype(jnp.bfloat16)
+
+    count = 4 * rows
+    vdim = value_w.shape[1] // heads
+    scale = math.log2(math.e) / math.sqrt(NOPE + rope)
+
+    @scoped("attend_start")
+    def attend_start():
         peak[...] = jnp.full_like(peak, -1e30)
         total[...] = jnp.zeros_like(total)
         acc[...] = jnp.zeros_like(acc)
-
-        def block(number, masked):
-            seen = lat[number].reshape(count, lat.shape[4])
-            keys = jnp.dot(seen, key_w[...], preferred_element_type=jnp.float32).astype(
+        value_t[...] = value_w[...].astype(jnp.float32).T.astype(jnp.bfloat16)
+        for h in range(heads):
+            keys_s[:, h * PAD + NOPE : (h + 1) * PAD] = jnp.zeros(
+                (count, PAD - NOPE), jnp.bfloat16
+            )
+
+    def attend_block(number, masked):
+        seen = lat[number, :, :, :, :kv_width].reshape(count, kv_width)
+        turned_key = lat[number, :, :, :, kv_width:].reshape(count, rope)
+        flat = jnp.dot(seen, key_w[...], preferred_element_type=jnp.float32)
+        vals = lax.dot_general(
+            value_t[...], seen, NT, preferred_element_type=jnp.float32
+        ).astype(jnp.bfloat16)
+        for h in range(heads):
+            keys_s[:, h * PAD : h * PAD + NOPE] = flat[:, h * NOPE : (h + 1) * NOPE].astype(
                 jnp.bfloat16
             )
-            vals = lax.dot_general(
-                value_w[...], seen, NT, preferred_element_type=jnp.float32
-            ).astype(jnp.bfloat16)
-            for h in range(heads):
-                score = (
-                    lax.dot_general(
-                        keys[:, h * PAD : (h + 1) * PAD],
-                        heads_q[:, h * PAD : (h + 1) * PAD],
-                        NT,
-                        preferred_element_type=jnp.float32,
-                    )
-                    * scale
+            keys_s[:, h * PAD + NOPE : h * PAD + NOPE + rope] = turned_key
+        for h in range(heads):
+            score = (
+                lax.dot_general(
+                    keys_s[:, h * PAD : (h + 1) * PAD],
+                    heads_q[:, h * PAD : (h + 1) * PAD],
+                    NT,
+                    preferred_element_type=jnp.float32,
                 )
-                if masked:
-                    key = lax.broadcasted_iota(jnp.int32, score.shape, 0)
-                    query = lax.broadcasted_iota(jnp.int32, score.shape, 1)
-                    score = jnp.where(key <= query, score, -1e30)
-                old = peak[h : h + 1, :]
-                new = jnp.maximum(old, jnp.max(score, axis=0, keepdims=True))
-                expo = jnp.exp2(score - new)
-                factor = jnp.exp2(old - new)
-                peak[h : h + 1, :] = new
-                total[h : h + 1, :] = total[h : h + 1, :] * factor + jnp.sum(
-                    expo, axis=0, keepdims=True
-                )
-                part_rows = slice(h * vdim, (h + 1) * vdim)
-                acc[part_rows, :] = acc[part_rows, :] * factor + jnp.dot(
-                    vals[part_rows, :], expo.astype(jnp.bfloat16), preferred_element_type=jnp.float32
-                )
-
-        @pl.loop(0, ep)
-        def _(number):
-            block(number, False)
-
-        block(ep, True)
+                * scale
+            )
+            if masked:
+                key = lax.broadcasted_iota(jnp.int32, score.shape, 0)
+                query = lax.broadcasted_iota(jnp.int32, score.shape, 1)
+                score = jnp.where(key <= query, score, -1e30)
+            old = peak[h : h + 1, :]
+            new = jnp.maximum(old, jnp.max(score, axis=0, keepdims=True))
+            expo = jnp.exp2(score - new)
+            factor = jnp.exp2(old - new)
+            peak[h : h + 1, :] = new
+            total[h : h + 1, :] = total[h : h + 1, :] * factor + jnp.sum(
+                expo, axis=0, keepdims=True
+            )
+            part_rows = slice(h * vdim, (h + 1) * vdim)
+            acc[part_rows, :] = acc[part_rows, :] * factor + jnp.dot(
+                vals[part_rows, :], expo.astype(jnp.bfloat16), preferred_element_type=jnp.float32
+            )
+
+    @scoped("attend_own")
+    def attend_own():
+        attend_block(ep, True)
+
+    @scoped("attend_side")
+    def attend_side():
+        @pl.when(ep % 2 == 1)
+        def _():
+            attend_block(ep - 1, False)
+
+    @scoped("attend_level")
+    def attend_level(k):
+        @pl.when(level >= k)
+        def _():
+            @pl.loop(0, 2)
+            def _(side):
+                attend_block((level - k) * 2 + side, False)
+
+    @scoped("combine")
+    def combine(s):
+        if s:
+            to_home(s).wait_recv()
+        group = partner(ep, s)
+        both = lax.dot_general(
+            shares[group],
+            back[group],
+            (((0,), (0,)), ((), ())),
+            preferred_element_type=jnp.float32,
+        )
+        blend[...] += both[:rows] + both[rows:]
+
+    @scoped("attend_end")
+    def attend_end():
         for h in range(heads):
             part_rows = slice(h * vdim, (h + 1) * vdim)
             attended[:, part_rows] = (acc[part_rows, :] / total[h : h + 1, :]).T.astype(
                 jnp.bfloat16
             )
 
+    @scoped("mix")
     def mix(owner_y, owner_core):
         start = pl.multiple_of((owner_y * 2 + owner_core) * rows, rows)
         return jnp.dot(
@@ -703,57 +856,98 @@
     mix_near = box.copy(mixed.at[2:4], mix_sib, mix_sem, 0, tp=1)
     mix_over = box.copy(mix_chip, mix_far, mix_sem, 1, tp=2)
 
-    for s in range(1, groups):
+    own_copy = pltpu.make_async_copy(outgoing.at[ep], recv.at[0, 0], load_sem.at[9])
+    lat_over.start()
+    lat_near.start()
+    q_over.start()
+    q_near.start()
+    loads[3].wait()
+    scope = jax.named_scope("prepare_rows")
+    scope.__enter__()
+    prepare_rows(
+        local,
+        main,
+        rest,
+        rows_in,
+        moe_gain,
+        routes,
+        route_weight,
+        outgoing,
+        shares,
+    )
+    scope.__exit__(None, None, None)
+    own_copy.start()
+    quarter = groups // 4
+    outer = range(quarter, steps)
+    inner = range(1, quarter)
+    for s in range(1, 2 * quarter + 2):
         dispatch(s).start()
     forward(0)
-    lat_over.start()
-    lat_near.start()
-    forward(1)
-    cross(0)
     lat_over.wait_recv()
     lat_near_over.start()
-    loads[4].wait()
     chain(0)
-    q_over.start()
-    q_near.start()
-    loads[0].wait()
-    loads[1].wait()
-    loads[2].wait()
-    loads[3].wait()
-    loads[5].wait()
-    for s in (2, 3):
+    for s in range(2 * quarter + 2, groups):
+        dispatch(s).start()
+    forward(1)
+    for one in loads[4:] + loads[:3] + [own_copy]:
+        one.wait()
+    q_over.wait_recv()
+    q_near_over.start()
+    cross(0)
+    attend_start()
+    blend[...] = jnp.zeros_like(blend)
+    for s in range(2, 2 * quarter):
         forward(s)
-    cross(1)
-    for k in range(steps):
-        compute(k)
-        for s in (2 * k + 2, 2 * k + 3):
-            if s < groups:
-                cross(s)
-        for s in (2 * k + 4, 2 * k + 5):
-            if s < groups:
-                forward(s)
-        if k == 0:
-            q_over.wait_recv()
-            q_near_over.start()
-            chain_side(0)
-        if k:
-            chain(k)
-        chip_sum(k)
-        if k:
-            finish(k - 1)
-            chain_side(k)
-    for k in range(steps, levels):
-        chain(k)
-        chain_side(k)
-    finish(steps - 1)
     q_near.wait_recv()
     q_near_over.wait_recv()
     project_queries()
+    cross(1)
+    compute(0)
+    forward(2 * quarter)
+    forward(2 * quarter + 1)
+    chain_side(0)
+    chain(1)
+    for k in inner:
+        cross(2 * k)
+        cross(2 * k + 1)
+        compute(k)
     lat_near.wait_recv()
     lat_near_over.wait_recv()
-    for k in range(levels):
-        chain_end(k)
-    attention()
+    attend_own()
+    for k in outer:
+        for s in (2 * k + 2, 2 * k + 3):
+            if s < groups:
+                forward(s)
+        number = k - quarter + 1
+        cross(2 * k)
+        cross(2 * k + 1)
+        compute(k)
+        chain_side(number)
+        if number + 1 < levels:
+            chain(number + 1)
+        chip_sum(k)
+        if k == quarter:
+            chain_end(0)
+            attend_side()
+            for one in (0, *inner):
+                chip_sum(one)
+    for k in (0, *inner):
+        for s in (2 * k, 2 * k + 1):
+            to_far(s).start()
+    chain_end(1)
+    attend_level(1)
+    for number, k in enumerate(outer):
+        finish(k)
+        if number + 2 < levels:
+            if number + 2 > len(outer):
+                chain_side(number + 2)
+            chain_end(number + 2)
+            attend_level(number + 2)
+    for number in range(len(outer) + 2, levels):
+        chain_side(number)
+        chain_end(number)
+        attend_level(number)
+    attend_end()
     mixed[2] = mix(y, 1 - core)
     mixed[3] = mix(1 - y, 1 - core)
     mix_near.start()
@@ -763,10 +957,18 @@
     mix_chip[...] = add_rounded(mixed[1], mix_sib[1])
     mix_over.start()
     mixed[0] = add_rounded(mixed[0], mix_sib[0])
+    for k in (0, *inner):
+        finish(k)
+    combine(0)
+    for k in outer:
+        combine(2 * k)
+        combine(2 * k + 1)
+    combine(1)
+    for s in range(2, 2 * quarter):
+        combine(s)
     mix_over.wait_recv()
-    mixed_out[...] = add_rounded(mixed[0], mix_far[...])
-    for s in range(1, groups):
-        to_home(s).wait_recv()
+    mixed_out[...] = mixed[0].astype(jnp.float32) + mix_far[...].astype(jnp.float32)
+    expert_out[...] = blend[...]
     for s in range(1, groups):
         dispatch(s).wait_send()
         to_home(s).wait_send()
@@ -778,14 +980,15 @@
         one.wait_send()
 
 
-def fused(
-    outgoing, lat, query, cos, sin, query_w, key_w, value_w, output_w, gate_w, up_w, down_w, sizes
-):
+def fused(groups, small, rows_in, weights, sizes):
     heads, rope, main, rest = sizes
-    groups, piece, depth = outgoing.shape
-    rows, lat_width = lat.shape
+    query_in, kv_in = small[0], small[1]
+    gate_w, up_w, down_w = weights[-3:]
+    depth = rows_in.shape[1]
+    rows, kv_width = kv_in.shape
     local = gate_w.shape[0]
-    pair = (2, piece, depth)
+    piece = local * (main + rest)
+    vdims = weights[3].shape[1]
     chunks = 8
     mains = chunks * main
     rests = chunks * local * rest
@@ -795,28 +998,35 @@
     levels = groups // 2
     sem = pltpu.SemaphoreType.DMA
     scratch = [
-        pltpu.VMEM(gate_w.shape, bf),
-        pltpu.VMEM(up_w.shape, bf),
-        pltpu.VMEM(down_w.shape, bf),
+        pltpu.VMEM(rows_in.shape, bf),
+        pltpu.VMEM((groups, piece, depth), bf),
+        pltpu.VMEM((groups, piece, depth), bf),
+        pltpu.VMEM((groups, piece, 2 * rows), bf),
+        pltpu.VMEM(rows_in.shape, fl),
+        *[pltpu.VMEM(one.shape, bf) for one in weights[:-3]],
+        pltpu.VMEM((vdims, kv_width), bf),
+        pltpu.VMEM((4 * rows, heads * PAD), bf),
+        *[pltpu.VMEM(one.shape, bf) for one in weights[-3:]],
         pltpu.VMEM((groups, 4, piece, depth), bf),
-        pltpu.VMEM((groups,) + pair, bf),
+        pltpu.VMEM((groups, 2, piece, depth), bf),
         pltpu.VMEM((groups, piece, depth), bf),
         pltpu.VMEM((groups, piece, depth), bf),
         pltpu.VMEM((groups, piece, depth), bf),
         pltpu.VMEM((mains + rests, depth), bf),
         pltpu.VMEM((rests, depth), fl),
-        pltpu.VMEM((groups, 2, 2, rows, lat_width), bf),
-        pltpu.VMEM((2, 2) + query.shape, bf),
+        pltpu.VMEM((groups, 2, 2, rows, kv_width + rope), bf),
+        pltpu.VMEM((rows, 2 * rope), fl),
+        pltpu.VMEM((2, 2) + query_in.shape, bf),
         pltpu.VMEM((4 * rows, heads * PAD), bf),
         pltpu.VMEM((heads, 4 * rows), fl),
         pltpu.VMEM((heads, 4 * rows), fl),
-        pltpu.VMEM((value_w.shape[0], 4 * rows), fl),
-        pltpu.VMEM((4 * rows, value_w.shape[0]), bf),
+        pltpu.VMEM((vdims, 4 * rows), fl),
+        pltpu.VMEM((4 * rows, vdims), bf),
         pltpu.VMEM((4, rows, depth), bf),
         pltpu.VMEM((2, rows, depth), bf),
         pltpu.VMEM((rows, depth), bf),
         pltpu.VMEM((rows, depth), bf),
-        sem((6,)),
+        sem((10,)),
         sem((2, groups)),
         sem((2, groups)),
         sem((2, groups)),
@@ -835,16 +1045,16 @@
     return pl.pallas_call(
         functools.partial(fused_kernel, heads, rope, main, rest),
         out_shape=(
-            jax.ShapeDtypeStruct(outgoing.shape, bf),
-            jax.ShapeDtypeStruct((rows, depth), bf),
+            jax.ShapeDtypeStruct((rows, depth), fl),
+            jax.ShapeDtypeStruct((rows, depth), fl),
         ),
-        in_specs=[vmem] * 9 + [hbm] * 3,
+        in_specs=[vmem] * len(small) + [hbm] * (1 + len(weights)),
         out_specs=(vmem, vmem),
         scratch_shapes=scratch,
         compiler_params=pltpu.CompilerParams(
-            collective_id=0, has_side_effects=True, vmem_limit_bytes=60 * 1024 * 1024
+            collective_id=0, has_side_effects=True, vmem_limit_bytes=62 * 1024 * 1024
         ),
-    )(outgoing, lat, query, cos, sin, query_w, key_w, value_w, output_w, gate_w, up_w, down_w)
+    )(*small, rows_in, *weights)
 
 
 def per_device(
@@ -882,6 +1092,8 @@
         and main % 16 == 0
         and local * rest % 8 == 0
         and heads * rope == 128
+        and 2 * rope == 128
+        and ep_size >= 4
     ):
         return plain_device(
             query_latent,
@@ -903,73 +1115,22 @@
             down_w,
         )
     half = rope // 2
-    group_rows = tok_rows * tp_size
-    freq = 1.0 / THETA ** (jnp.arange(half, dtype=jnp.float32) * 2.0 / rope)
-    first_pos = lax.axis_index("ep") * group_rows
-    positions = first_pos + jnp.arange(group_rows, dtype=jnp.int32)
-    own = lax.axis_index("tp") * tok_rows + first_pos + jnp.arange(tok_rows, dtype=jnp.int32)
-    own_angle = own.astype(jnp.float32)[:, None] * jnp.tile(freq, 2)[None, :]
-    keys = rope_key.astype(jnp.float32)
-    turned = jnp.concatenate([-keys[:, half:], keys[:, :half]], axis=-1)
-    key_rot = (keys * jnp.cos(own_angle) + turned * jnp.sin(own_angle)).astype(jnp.bfloat16)
-    own_latents = jnp.concatenate([rms_scale(kv_latent, kv_gain), key_rot], axis=1)
-    own_query = rms_scale(query_latent, query_gain)
-    angle = positions.astype(jnp.float32)[:, None] * jnp.tile(freq, 2 * heads)[None, :]
-    turned_w = []
-    for h in range(heads):
-        turned_w.append(-query_rope_w[:, h * rope + half : (h + 1) * rope])
-        turned_w.append(query_rope_w[:, h * rope : h * rope + half])
-    query_w = jnp.concatenate([query_nope_w, query_rope_w] + turned_w, axis=1)
-    key_w = jnp.concatenate(
-        [
-            jnp.concatenate(
-                [
-                    jnp.pad(key_up_w[:, h * NOPE : (h + 1) * NOPE], ((0, 0), (0, PAD - NOPE))),
-                    jnp.pad(
-                        jnp.eye(rope, dtype=jnp.bfloat16),
-                        ((0, 0), (NOPE + h * rope, PAD - NOPE - (h + 1) * rope)),
-                    ),
-                ],
-                axis=0,
-            )
-            for h in range(heads)
-        ],
-        axis=1,
-    )
-    value_w = jnp.pad(value_up_w.T, ((0, 0), (0, rope)))
-    floats = expert_in.astype(jnp.float32)
-    center = floats - jnp.mean(floats, axis=-1, keepdims=True)
-    variance = jnp.mean(center * center, axis=-1, keepdims=True)
-    normed_in = (center * lax.rsqrt(variance + 1e-05) * moe_gain).astype(jnp.bfloat16)
-    hits = route(routes, experts, local, capacity)
-    select = functools.reduce(jnp.logical_or, hits).astype(jnp.bfloat16)
-    outgoing = (
-        lax.dot_general(select, normed_in, (((0,), (0,)), ((), ())), preferred_element_type=jnp.float32)
-        .astype(jnp.bfloat16)
-        .reshape(ep_size, local * capacity, width)
-    )
-    back, mixer_out = fused(
-        outgoing,
-        own_latents,
-        own_query,
-        jnp.cos(angle),
-        jnp.sin(angle),
-        query_w,
-        key_w,
-        value_w,
-        output_w,
-        gate_w,
-        up_w,
-        down_w,
-        (heads, rope, main, rest),
-    )
-    back = back.reshape(experts * capacity, width)
-    weights = route_weight / jnp.sum(route_weight, axis=-1, keepdims=True)
-    mix = sum(jnp.where(hit, weights[:, k : k + 1], 0.0) for k, hit in enumerate(hits))
-    high = mix.astype(jnp.bfloat16)
-    low = (mix - high.astype(jnp.float32)).astype(jnp.bfloat16)
-    both = jnp.dot(jnp.concatenate([high, low], axis=0), back, preferred_element_type=jnp.float32)
-    return mixer_out, (both[:tok_rows] + both[tok_rows:]).astype(jnp.bfloat16)
+    exponent = np.arange(half, dtype=np.float32) * np.float32(2.0) / np.float32(rope)
+    freq = np.float32(1.0) / np.float32(THETA) ** exponent
+    small = (
+        query_latent,
+        kv_latent,
+        rope_key.T,
+        query_gain,
+        kv_gain,
+        jnp.asarray(np.tile(freq, 4)[None, :]),
+        moe_gain,
+        routes.T,
+        route_weight.T,
+    )
+    big = (query_nope_w, query_rope_w, key_up_w, value_up_w, output_w, gate_w, up_w, down_w)
+    mixed, blend = fused(ep_size, small, expert_in, big, (heads, rope, main, rest))
+    return mixed.astype(jnp.bfloat16), blend.astype(jnp.bfloat16)
 
 
 def solution(mesh):

time: 126 us -> 102 us (0.81)
  the two profiles are of different devices: /device:TPU:31 before, /device:TPU:0 now
where the time goes in v2:
time: 102 us
  Pallas kernels  96.8 us (95%)
  other arithmetic  4.17 us (4%)
    pallas_call x1, Pallas kernels, fused(): pl.pallas_call(functools.partial(fused_kernel, heads, rope, main, rest),...  96.8 us
    convert_element_type x2, other arithmetic, per_device(): return (mixed.astype(jnp.bfloat16), blend.astype(jnp.bfloat16))  4.17 us

profile of v2, /device:TPU:0, one launch (start us, length us, event | category | flops | bytes accessed | tf_op | source)
XLA Modules:
  0.0 101.6 jit_solution(18139239351446866054)
XLA Ops:
  0.6 96.8 %shard_map.185 = (f32[128,2048]{1,0:T(8,128)}, f32[128,2048]{1,0:T(8,128)}) custom-call(bf16[128,768]{1,0:T(8,128)(2,1)} %query_in.1, bf16[128,512]{1,0:T(8,128)(2,1)} %kv_in.1, bf16[64,128]{1,0:T(8,128)(2,1)} %bitcast.3, f32[768]{0:T(1024)} %query_gain.1, f32[512]{0:T(512)} %kv_gain.1, f32[1,128]{1,0:T(1,128)} %constant.2.clone.freq, f32[2048]{0:T(1024)} %moe_gain.1, ...), custom_call_target="tpu_custom_call" | custom-call | tf_op jit(solution)/shard_map/pallas_call | solution.py:1045
  97.5 2.1 %convert_element_type.6 = bf16[128,2048]{1,0:T(8,128)(2,1)} convert(f32[128,2048]{1,0:T(8,128)} %get-tuple-element.4) | non-fusion elementwise | flops 262144 | bytes 1572864 | tf_op jit(solution)/shard_map/convert_element_type | solution.py:1133
  99.5 2.1 %convert_element_type.7 = bf16[128,2048]{1,0:T(8,128)(2,1)} convert(f32[128,2048]{1,0:T(8,128)} %get-tuple-element.5) | non-fusion elementwise | flops 262144 | bytes 1572864 | tf_op jit(solution)/shard_map/convert_element_type | solution.py:1133

commit v3 on v2

--- a/solution.py
+++ b/solution.py
@@ -922,18 +922,20 @@
         cross(2 * k)
         cross(2 * k + 1)
         compute(k)
+        if number == 1:
+            for one in (0, *inner):
+                chip_sum(one)
+        chip_sum(k)
+        if number == len(outer):
+            for one in (0, *inner):
+                for s in (2 * one, 2 * one + 1):
+                    to_far(s).start()
         chain_side(number)
         if number + 1 < levels:
             chain(number + 1)
-        chip_sum(k)
-        if k == quarter:
+        if number == 1:
             chain_end(0)
             attend_side()
-            for one in (0, *inner):
-                chip_sum(one)
-    for k in (0, *inner):
-        for s in (2 * k, 2 * k + 1):
-            to_far(s).start()
     chain_end(1)
     attend_level(1)
     for number, k in enumerate(outer):

time: 102 us -> 103 us (level)
  Pallas kernels: 96.8 us -> 98.3 us
    pallas_call x1, Pallas kernels: 96.8 us -> 98.3 us  [fused(): pl.pallas_call(functools.partial(fused_kernel, heads, rope, main, rest),...]
where the time goes in v3:
time: 103 us
  Pallas kernels  98.3 us (95%)
  other arithmetic  4.17 us (4%)
    pallas_call x1, Pallas kernels, fused(): pl.pallas_call(functools.partial(fused_kernel, heads, rope, main, rest),...  98.3 us
    convert_element_type x2, other arithmetic, per_device(): return (mixed.astype(jnp.bfloat16), blend.astype(jnp.bfloat16))  4.17 us

profile of v3, /device:TPU:0, one launch (start us, length us, event | category | flops | bytes accessed | tf_op | source)
XLA Modules:
  0.0 103.1 jit_solution(10944536293202369580)
XLA Ops:
  0.6 98.3 %shard_map.185 = (f32[128,2048]{1,0:T(8,128)}, f32[128,2048]{1,0:T(8,128)}) custom-call(bf16[128,768]{1,0:T(8,128)(2,1)} %query_in.1, bf16[128,512]{1,0:T(8,128)(2,1)} %kv_in.1, bf16[64,128]{1,0:T(8,128)(2,1)} %bitcast.3, f32[768]{0:T(1024)} %query_gain.1, f32[512]{0:T(512)} %kv_gain.1, f32[1,128]{1,0:T(1,128)} %constant.2.clone.freq, f32[2048]{0:T(1024)} %moe_gain.1, ...), custom_call_target="tpu_custom_call" | custom-call | tf_op jit(solution)/shard_map/pallas_call | solution.py:1047
  99.0 2.1 %convert_element_type.6 = bf16[128,2048]{1,0:T(8,128)(2,1)} convert(f32[128,2048]{1,0:T(8,128)} %get-tuple-element.4) | non-fusion elementwise | flops 262144 | bytes 1572864 | tf_op jit(solution)/shard_map/convert_element_type | solution.py:1135
  101.0 2.1 %convert_element_type.7 = bf16[128,2048]{1,0:T(8,128)(2,1)} convert(f32[128,2048]{1,0:T(8,128)} %get-tuple-element.5) | non-fusion elementwise | flops 262144 | bytes 1572864 | tf_op jit(solution)/shard_map/convert_element_type | solution.py:1135
